TPU v7x, 32 devices: a whole 2x2x4 slice. The times are simulated.
32 devices in a mesh: sp: 16 (over z, y, x), tp: 2 (over core).
Axes of the slice: x: 2, y: 2, z: 4, core: 2. Of those that a mesh axis runs over, the one named last changes fastest.
Arguments:
- tokens: bfloat16 [6144, 2048], P('sp', 'tp'), may hold values from -1620 to 1620
- input_norm_gain: float32 [2048], replicated, may hold values from 0.1 to 1.9
- outer_gate_weight: bfloat16 [2048, 1024], P(None, 'tp'), may hold values from -0.125 to 0.125
- inner_gate_weight: bfloat16 [2048, 1024], P(None, 'tp'), may hold values from -0.125 to 0.125
- convolution_input_weight: bfloat16 [2048, 1024], P(None, 'tp'), may hold values from -0.125 to 0.125
- convolution_kernel_taps: bfloat16 [3, 1024], P(None, 'tp'), may hold values from -3 to 3
- query_weight_matrix: bfloat16 [2048, 512], P(None, 'tp'), may hold values from -0.125 to 0.125
- key_weight_matrix: bfloat16 [2048, 512], P(None, 'tp'), may hold values from -0.125 to 0.125
- value_weight_matrix: bfloat16 [2048, 1024], P(None, 'tp'), may hold values from -0.125 to 0.125
- forget_gate_weight: bfloat16 [2048, 512], P(None, 'tp'), may hold values from -0.125 to 0.125
- attention_gate_weight: bfloat16 [2048, 1024], P(None, 'tp'), may hold values from -0.125 to 0.125
- forget_gate_bias: float32 [512], P('tp'), may hold values from -1.5 to 10
- extra_logarithm_decay: float32 [6144, 16], P('sp', 'tp'), may hold values from -0.72 to 0
- initial_head_state: float32 [16, 32, 64], P('tp'), may hold values from -768 to 768
- head_norm_gain: float32 [64], replicated, may hold values from 0.1 to 1.9
- convolution_output_weight: bfloat16 [1024, 2048], P('tp'), may hold values from -0.125 to 0.125
- attention_output_weight: bfloat16 [1024, 2048], P('tp'), may hold values from -0.125 to 0.125
Outputs:
- mixed: bfloat16 [6144, 2048], P(('sp', 'tp'))
All inputs are finite; a program needn't handle non-finite values.
Results may differ from a plain program's by a relative error of at most 0.017.
Values may be sent and summed in bfloat16 or wider, within the bound.
No kernel may reach another device: no remote copies, remote signals or barrier semaphores. Data moves between devices by JAX's collectives and lax.ppermute only.
A program may use at most 128 MiB of HBM per device.

v0:
```python
import jax
import jax.numpy as jnp
from jax import lax
from jax.sharding import PartitionSpec as P

BLOCK = 64


NORM_EPS = 1e-06
GATE_SOFTNESS = 16.0


def from_behind(block, axis, distance):
    devices = range(lax.axis_size(axis))
    route = [(i - distance, i) for i in devices if i - distance in devices]
    return lax.ppermute(block, axis, route)


def prefix(part, axis, combine, identity):
    place = lax.axis_index(axis)
    gathered = jax.tree.map(lambda a: lax.all_gather(a, axis), part)
    state = jax.tree.map(lambda a, e: jnp.zeros_like(a) + jnp.asarray(e, a.dtype), part, identity)

    def one(turn, state):
        return combine(
            state, jax.tree.map(lambda a: lax.dynamic_index_in_dim(a, turn, 0, False), gathered)
        )

    return lax.fori_loop(0, place, one, state)


def block_terms(queries, key_rows, values, logarithm_decay):
    cumulative = jnp.cumsum(logarithm_decay, axis=1)
    last_log = cumulative[:, -1:]
    query_g = queries * jnp.exp(cumulative)
    key_g = key_rows * jnp.exp(-cumulative)
    scores = jnp.einsum("nihd,njhd->nhij", query_g, key_g, precision=lax.Precision.HIGHEST)
    width = queries.shape[1]
    causal = jnp.arange(width)[:, None] >= jnp.arange(width)[None, :]
    scores = jnp.where(causal, scores, 0.0)
    inner = jnp.einsum("nhij,njhe->nihe", scores, values, precision=lax.Precision.HIGHEST)
    key_decayed = key_rows * jnp.exp(last_log - cumulative)
    update = jnp.einsum("nchd,nche->nhde", key_decayed, values, precision=lax.Precision.HIGHEST)
    return (query_g, inner, update, last_log[:, 0])


def carry_step(state, inputs):
    block_decay, update = inputs
    return (block_decay[..., None] * state + update, state)


def chain_join(earlier, later):
    return (earlier[0] * later[0], later[0][..., None] * earlier[1] + later[1])


def on_device(
    tokens,
    input_norm_gain,
    outer_gate_weight,
    inner_gate_weight,
    convolution_input_weight,
    convolution_kernel_taps,
    query_weight_matrix,
    key_weight_matrix,
    value_weight_matrix,
    forget_gate_weight,
    attention_gate_weight,
    forget_gate_bias,
    extra_logarithm_decay,
    initial_head_state,
    head_norm_gain,
    convolution_output_weight,
    attention_output_weight,
):
    number_of_rows = tokens.shape[0]
    number_of_heads, key_channel_count, value_dim = initial_head_state.shape
    weights = (
        outer_gate_weight,
        inner_gate_weight,
        convolution_input_weight,
        query_weight_matrix,
        key_weight_matrix,
        value_weight_matrix,
        forget_gate_weight,
        attention_gate_weight,
    )
    whole_rows = lax.all_gather(tokens, "tp", axis=1, tiled=True).astype(jnp.float32)
    power = jnp.mean(whole_rows * whole_rows, axis=1, keepdims=True)
    normed = (whole_rows * lax.rsqrt(power + NORM_EPS) * input_norm_gain).astype(jnp.bfloat16)
    sums = tuple(
        (jnp.dot(normed, weight, preferred_element_type=jnp.float32) for weight in weights)
    )
    conv_b, conv_c, conv_h, query, key_proj, value, forget_preactivation, out_gate = (
        term.astype(jnp.bfloat16) for term in sums
    )
    product = (conv_c.astype(jnp.float32) * conv_h.astype(jnp.float32)).astype(jnp.bfloat16)
    tap_count = convolution_kernel_taps.shape[0]
    previous = from_behind(product[number_of_rows - tap_count + 1 :], "sp", 1)
    padded = jnp.concatenate([previous, product], axis=0)
    conv = jnp.zeros(product.shape, jnp.float32)
    for tap_index in range(tap_count):
        conv = conv + convolution_kernel_taps[tap_index].astype(jnp.float32) * padded[
            tap_index : tap_index + number_of_rows
        ].astype(jnp.float32)
    conv_out = (conv_b.astype(jnp.float32) * conv).astype(jnp.bfloat16)
    logarithm_decay = (
        jax.nn.log_sigmoid(forget_preactivation.astype(jnp.float32) + forget_gate_bias)
        / GATE_SOFTNESS
    )
    logarithm_decay = (
        logarithm_decay.reshape(number_of_rows, number_of_heads, key_channel_count)
        + extra_logarithm_decay[:, :, None]
    )
    n_blocks = number_of_rows // BLOCK
    queries = (query.astype(jnp.float32) * key_channel_count ** (-0.5)).reshape(
        n_blocks, BLOCK, number_of_heads, key_channel_count
    )
    key_rows = key_proj.astype(jnp.float32).reshape(
        n_blocks, BLOCK, number_of_heads, key_channel_count
    )
    values = value.astype(jnp.float32).reshape(n_blocks, BLOCK, number_of_heads, value_dim)
    query_g, inner, update, block_log = block_terms(
        queries,
        key_rows,
        values,
        logarithm_decay.reshape(n_blocks, BLOCK, number_of_heads, key_channel_count),
    )
    zero_state = jnp.zeros((number_of_heads, key_channel_count, value_dim), jnp.float32)
    local_final, entering = lax.scan(carry_step, zero_state, (jnp.exp(block_log), update))
    exclusive = jnp.cumsum(block_log, axis=0) - block_log
    device_decay = jnp.exp(jnp.sum(block_log, axis=0))
    prefix_decay, prefix_state = prefix(
        (device_decay, local_final), "sp", chain_join, (jnp.ones_like(device_decay), zero_state)
    )
    incoming = prefix_state + prefix_decay[..., None] * initial_head_state
    entering = entering + jnp.exp(exclusive)[..., None] * incoming[None]
    outer = jnp.einsum("nchd,nhde->nche", query_g, entering, precision=lax.Precision.HIGHEST)
    raw = (inner + outer).reshape(number_of_rows, number_of_heads, value_dim)
    raw = raw * lax.rsqrt(jnp.mean(raw * raw, axis=2, keepdims=True) + NORM_EPS) * head_norm_gain
    gate_values = jax.nn.silu(out_gate.astype(jnp.float32)).reshape(
        number_of_rows, number_of_heads, value_dim
    )
    attn_out = (
        (raw * gate_values)
        .reshape(number_of_rows, number_of_heads * value_dim)
        .astype(jnp.bfloat16)
    )
    return lax.psum_scatter(
        (
            jnp.dot(conv_out, convolution_output_weight, preferred_element_type=jnp.float32)
            + jnp.dot(attn_out, attention_output_weight, preferred_element_type=jnp.float32)
        ).astype(jnp.bfloat16),
        "tp",
        scatter_dimension=0,
        tiled=True,
    )


def solution(mesh):
    placed = (
        P("sp", "tp"),
        P(),
        P(None, "tp"),
        P(None, "tp"),
        P(None, "tp"),
        P(None, "tp"),
        P(None, "tp"),
        P(None, "tp"),
        P(None, "tp"),
        P(None, "tp"),
        P(None, "tp"),
        P("tp"),
        P("sp", "tp"),
        P("tp", None, None),
        P(),
        P("tp", None),
        P("tp", None),
    )
    return jax.shard_map(
        on_device, mesh=mesh, in_specs=placed, out_specs=P(("sp", "tp"), None), check_vma=False
    )
```

profile of v0, /device:TPU:0, one launch (start us, length us, event | category | flops | bytes accessed | tf_op | source)
XLA Modules:
  0.0 176.2 jit_solution(7418654759086508791)
XLA Ops:
  6.5 0.7 all-gather.5.cloned.1.call-update
  7.3 0.7 mul.190
  8.1 0.8 add.99
  8.9 0.8 slice_convert_fusion.2
  9.7 11.8 %all-gather.5.cloned.1.call-done = bf16[384,2048]{1,0:T(8,128)(2,1)} async-done(((bf16[384,1024]{1,0:T(8,128)(2,1)}), bf16[384,2048]{1,0:T(8,128)(2,1)}) %all-gather.5.cloned.1.call-update) | async-done | bytes 1572880 | tf_op jit(solution)/shard_map/all_gather | solution.py:87
  21.4 1.9 %fusion = f32[384]{0:T(512)S(1)} fusion(bf16[384,2048]{1,0:T(8,128)(2,1)} %all-gather.5.cloned.1.call-done), kind=kLoop, calls=%fused_computation.7 | loop fusion | flops 2358912 | bytes 1574400 | tf_op jit(solution)/shard_map/reduce_sum | solution.py:88
  23.4 2.0 %fusion.42 = f32[384,256]{1,0:T(8,128)S(1)} fusion(bf16[2048,256]{1,0:T(8,128)(2,1)} %param.30, f32[256]{0:T(256)S(1)} %copy-done.13, bf16[384,2048]{1,0:T(8,128)(2,1)S(1)} %copy-done.5, f32[2048]{0:T(1024)S(1)} %copy-done.12, f32[384]{0:T(512)S(1)} %add_rsqrt_fusion.1), kind=kOutput, calls=%fused_computation.68 | convolution fusion | flops 406978560 | bytes 3025408 | tf_op jit(solution)/shard_map/dot_general | solution.py:91
  25.4 0.9 copy.52
  26.4 1.2 reshape.85
  27.6 1.1 broadcast_add_fusion
  28.6 2.9 %copy.53 = f32[6,64,8,32]{3,2,1,0:T(8,128)} copy(f32[6,64,8,32]{1,0,3,2:T(8,128)} %broadcast_add_fusion) | data formatting | bytes 786432 | tf_op jit(solution)/shard_map/add | solution.py:111
  31.5 1.6 fusion.66
  33.2 1.1 copy-done.4
  34.3 2.6 %convolution_convert_fusion.1 = bf16[384,512]{1,0:T(8,128)(2,1)S(1)} fusion(bf16[2048,512]{1,0:T(8,128)(2,1)} %param.29, bf16[384,2048]{1,0:T(8,128)(2,1)S(1)} %copy-done.6, f32[2048]{0:T(1024)S(1)} %copy-done.12, f32[384]{0:T(512)S(1)} %add_rsqrt_fusion.1), kind=kOutput, calls=%fused_computation.24 | convolution fusion | flops 808648704 | bytes 4072960 | tf_op jit(solution)/shard_map/dot_general | solution.py:91
  37.4 2.6 %fusion.17 = f32[384,256]{1,0:T(8,128)S(1)} fusion(bf16[2048,256]{1,0:T(8,128)(2,1)} %param.28, bf16[384,2048]{1,0:T(8,128)(2,1)} %all-gather.5.cloned.1.call-done, f32[2048]{0:T(1024)S(1)} %copy-done.12, f32[384]{0:T(512)S(1)} %add_rsqrt_fusion.1), kind=kOutput, calls=%fused_computation.37 | convolution fusion | flops 405995520 | bytes 3024384 | tf_op jit(solution)/shard_map/dot_general | solution.py:91
  40.0 1.5 reshape.97
  41.5 2.3 %fusion.22 = f32[384,256]{1,0:T(8,128)S(1)} fusion(bf16[2048,256]{1,0:T(8,128)(2,1)} %param.27, bf16[384,2048]{1,0:T(8,128)(2,1)} %all-gather.5.cloned.1.call-done, f32[2048]{0:T(1024)S(1)} %copy-done.12, f32[384]{0:T(512)S(1)} %add_rsqrt_fusion.1), kind=kOutput, calls=%fused_computation.44 | convolution fusion | flops 406093824 | bytes 3024384 | tf_op jit(solution)/shard_map/dot_general | solution.py:91
  43.9 1.5 reshape.96
  45.4 4.6 %exponential_multiply_fusion = (f32[6,64,8,32]{3,2,1,0:T(8,128)S(1)}, f32[6,64,8,32]{3,2,1,0:T(8,128)}, f32[6,64,8,32]{3,2,1,0:T(8,128)}) fusion(f32[6,64,8,32]{3,2,1,0:T(8,128)} %reshape.97, f32[6,64,8,32]{3,2,1,0:T(8,128)} %copy-done.4, f32[6,8,32]{2,1,0:T(8,128)S(1)} %get-tuple-element.116, f32[6,64,8,32]{3,2,1,0:T(8,128)} %reshape.96), kind=kLoop, calls=%fused_computation.17 | loop fusion | flops 491520 | bytes 2365440 | tf_op jit(solution)/shard_map/mul | solution.py:42
  50.0 2.3 %fusion.3 = f32[6,8,32,64]{3,2,1,0:T(8,128)} fusion(f32[6,64,8,32]{3,2,1,0:T(8,128)S(1)} %get-tuple-element.113, bf16[6,64,8,64]{3,2,1,0:T(8,128)(2,1)S(1)} %reshape.83), kind=kOutput, calls=%fused_computation.11 | convolution fusion | flops 75497472 | bytes 1179648 | tf_op jit(solution)/shard_map/nchd,nche->nhde/dot_general | solution.py:43
  52.3 10.3 %while.26 = (s32[]{:T(128)}, f32[8,32,64]{2,1,0:T(8,128)S(1)}, f32[6,8,32,64]{3,2,1,0:T(8,128)}, f32[6,8,32]{2,1,0:T(8,128)S(1)}, f32[6,8,32,64]{3,2,1,0:T(8,128)}, /*index=5*/s32[]{:T(128)}, s32[]{:T(128)}) while((s32[]{:T(128)}, f32[8,32,64]{2,1,0:T(8,128)S(1)}, f32[6,8,32,64]{3,2,1,0:T(8,128)}, f32[6,8,32]{2,1,0:T(8,128)S(1)}, ...), condition=%wide.region_3.4_spmd.clone, body=%wide.region_2.3_spmd.clone.sunk | while | flops 65539 | bytes 396396 | solution.py:129
  52.3 0.7 bitcast_dynamic-update-slice_fusion.2
  53.0 1.0 bitcast_add_fusion.5
  54.0 0.7 bitcast_dynamic-update-slice_fusion.2
  54.7 1.0 bitcast_add_fusion.5
  55.8 0.7 bitcast_dynamic-update-slice_fusion.2
  56.4 1.0 bitcast_add_fusion.5
  57.5 0.7 bitcast_dynamic-update-slice_fusion.2
  58.2 1.0 bitcast_add_fusion.5
  59.2 0.7 bitcast_dynamic-update-slice_fusion.2
  59.9 1.0 bitcast_add_fusion.5
  61.0 0.7 bitcast_dynamic-update-slice_fusion.2
  61.6 1.0 bitcast_add_fusion.5
  63.4 3.2 %fusion.13 = f32[384,512]{1,0:T(8,128)S(1)} fusion(bf16[2048,512]{1,0:T(8,128)(2,1)} %param.24, bf16[384,2048]{1,0:T(8,128)(2,1)} %all-gather.5.cloned.1.call-done, f32[2048]{0:T(1024)S(1)} %copy-done.12, f32[384]{0:T(512)S(1)} %add_rsqrt_fusion.1), kind=kOutput, calls=%fused_computation.30 | convolution fusion | flops 808845312 | bytes 4466176 | tf_op jit(solution)/shard_map/dot_general | solution.py:91
  66.7 1.0 fusion.12
  67.7 3.8 %collective-permute-start = (bf16[2,512]{1,0:T(2,128)(2,1)S(1)}, bf16[2,512]{1,0:T(2,128)(2,1)S(1)}, u32[]{:S(2)}, u32[]{:S(2)}) collective-permute-start(bf16[2,512]{1,0:T(2,128)(2,1)S(1)} %slice.28), channel_id=1, source_target_pairs={{0,2},{2,4},{4,6},{6,8},{8,10},{10,12},{12,14},{14,16},{16,18},{18... | collective-permute-start | bytes 6152 | tf_op jit(solution)/shard_map/ppermute | solution.py:16
  71.6 1.9 %copy.57 = f32[6,64,8,32]{1,3,2,0:T(8,128)S(1)} copy(f32[6,64,8,32]{3,2,1,0:T(8,128)} %get-tuple-element.117) | data formatting | bytes 786432 | tf_op jit(solution)/shard_map/mul | solution.py:35
  73.5 1.0 fusion.23
  74.5 4.4 %fusion.5 = f32[6,8,64,64]{3,2,1,0:T(8,128)S(1)} fusion(f32[6,64,8,32]{1,3,2,0:T(8,128)S(1)} %copy.57, f32[6,64,8,32]{3,2,1,0:T(8,128)} %get-tuple-element.114), kind=kOutput, calls=%fused_computation.13 | convolution fusion | flops 75497472 | bytes 1572864 | tf_op jit(solution)/shard_map/nihd,njhd->nhij/dot_general | solution.py:37
  78.8 2.7 %fusion.7 = f32[6,8,64,64]{3,2,1,0:T(8,128)} fusion(f32[6,8,64,64]{3,2,1,0:T(8,128)S(1)} %fusion.5, pred[64,64]{1,0:T(8,128)(4,1)S(1)} %iota_compare_fusion, bf16[6,64,8,64]{3,2,1,0:T(8,128)(2,1)S(1)} %copy-done.3), kind=kOutput, calls=%fused_computation.18 | convolution fusion | flops 151191552 | bytes 1970176 | tf_op jit(solution)/shard_map/nhij,njhe->nihe/dot_general | solution.py:41
  81.5 39.2 %all-gather = f32[128,32]{1,0:T(8,128)S(1)} all-gather(f32[8,32]{1,0:T(8,128)S(1)} %exp.47), channel_id=2, replica_groups=mesh['sp'=16,'tp'=2] {'sp'}, dimensions={0}, use_global_device_ids=true | all-gather | bytes 17408 | tf_op jit(solution)/shard_map/all_gather | solution.py:21
  120.7 6.1 %fusion.24 = f32[384,2048]{1,0:T(8,128)} fusion(bf16[512,2048]{1,0:T(8,128)(2,1)S(1)} %copy-done, bf16[2048,512]{1,0:T(8,128)(2,1)} %param.23, bf16[384,512]{1,0:T(8,128)(2,1)} %copy-done.10, bf16[2,512]{1,0:T(2,128)(2,1)S(1)} %collective-permute-done, f32[512]{0:T(512)S(1)} %bitcast.57, f32[512]{0:T(512)S(1)} %bitcast.58, f32[512]{0:T(512)S(1)} %bitcast.56, ...), kind=kOutput, calls=%fused_computation.47 | convolution fusion | flops 1617297408 | bytes 9324032 | tf_op jit(solution)/shard_map/dot_general | solution.py:150
  127.8 5.7 %multiply_reduce_fusion = (f32[6,64,8]{1,2,0:T(8,128)S(1)}, f32[6,64,8,64]{1,3,2,0:T(8,128)}) fusion(f32[6,8,64,64]{3,2,1,0:T(8,128)} %fusion.7, f32[6,64,8,32]{1,3,2,0:T(8,128)S(1)} %copy.57, f32[6,8,32,64]{3,2,1,0:T(8,128)} %get-tuple-element.67, f32[8,32,64]{2,1,0:T(8,128)S(1)} %multiply_add_fusion, f32[6,8,32]{2,1,0:T(8,128)S(1)} %fusion.23), kind=kOutput, calls=%fused_computation.15 | convolution fusion | flops 76280832 | bytes 2443264 | tf_op jit(solution)/shard_map/nchd,nhde->nche/dot_general | solution.py:137
  133.7 1.2 copy.66
  134.9 3.0 %copy.64 = f32[6,64,8,64]{3,2,1,0:T(8,128)} copy(f32[6,64,8,64]{1,3,2,0:T(8,128)} %get-tuple-element.122) | data formatting | bytes 1572864 | tf_op jit(solution)/shard_map/add | solution.py:138
  137.9 2.6 %reshape.88 = f32[384,512]{1,0:T(8,128)} reshape(f32[6,64,8,64]{3,2,1,0:T(8,128)} %copy.64) | data formatting | bytes 1572864 | tf_op jit(solution)/shard_map/reshape | solution.py:138
  140.6 7.0 %add_convert_fusion = bf16[384,2048]{1,0:T(8,128)(2,1)} fusion(f32[384,2048]{1,0:T(8,128)} %fusion.24, bf16[512,2048]{1,0:T(8,128)(2,1)} %param.37, bf16[2048,512]{1,0:T(8,128)(2,1)} %param.31, f32[384,512]{1,0:T(8,128)} %reshape.88, f32[384,512]{1,0:T(8,128)S(1)} %copy-done.8, f32[512]{0:T(512)S(1)} %mul.191, ...), kind=kOutput, calls=%fused_computation.10 | convolution fusion | flops 1617297408 | bytes 12070400 | tf_op jit(solution)/shard_map/dot_general | solution.py:151
  147.6 22.0 %reduce-scatter.2.cloned.1.call-done = bf16[192,2048]{1,0:T(8,128)(2,1)} async-done(((bf16[384,2048]{1,0:T(8,128)(2,1)}), bf16[192,2048]{1,0:T(8,128)(2,1)}) %reduce-scatter.2.cloned.1.call-update) | async-done | bytes 786448 | tf_op jit(solution)/shard_map/reduce_scatter | solution.py:148
  (58 shorter events, 2.5 us)
Async XLA Ops:
  6.5 114.1 %copy-start = (bf16[512,2048]{1,0:T(8,128)(2,1)S(1)}, bf16[512,2048]{1,0:T(8,128)(2,1)}, u32[]{:S(2)}) copy-start(bf16[512,2048]{1,0:T(8,128)(2,1)} %param.36) | copy-start | bytes 6291460
  6.5 16.8 %copy-start.12 = (f32[2048]{0:T(1024)S(1)}, f32[2048]{0:T(1024)}, u32[]{:S(2)}) copy-start(f32[2048]{0:T(1024)} %param.22) | copy-start | bytes 24580
  6.5 16.8 %copy-start.13 = (f32[256]{0:T(256)S(1)}, f32[256]{0:T(256)}, u32[]{:S(2)}) copy-start(f32[256]{0:T(256)} %param.32) | copy-start | bytes 3076
  6.5 14.9 %all-gather.5.cloned.1.call-start = ((), (), s32[]{:S(2)}) async-start(), calls=%async_computation.1 | async-start | bytes 2359296 | tf_op jit(solution)/shard_map/all_gather | solution.py:87
  7.3 119.5 %all-gather.7.cloned.1.call-start = ((), (), s32[]{:S(2)}) async-start(), calls=%async_computation.3 | async-start | bytes 2228224 | tf_op jit(solution)/shard_map/all_gather | solution.py:21
  21.4 1.9 %copy-start.5 = (bf16[384,2048]{1,0:T(8,128)(2,1)S(1)}, bf16[384,2048]{1,0:T(8,128)(2,1)}, u32[]{:S(2)}) copy-start(bf16[384,2048]{1,0:T(8,128)(2,1)} %all-gather.5.cloned.1.call-done) | copy-start | bytes 4718596
  31.5 2.8 %copy-start.6 = (bf16[384,2048]{1,0:T(8,128)(2,1)S(1)}, bf16[384,2048]{1,0:T(8,128)(2,1)}, u32[]{:S(2)}) copy-start(bf16[384,2048]{1,0:T(8,128)(2,1)} %all-gather.5.cloned.1.call-done) | copy-start | bytes 4718596
  33.2 1.2 copy-start.4
  37.3 12.6 %copy-start.2 = (bf16[6,64,8,64]{3,2,1,0:T(8,128)(2,1)}, bf16[6,64,8,64]{3,2,1,0:T(8,128)(2,1)S(1)}, u32[]{:S(2)}) copy-start(bf16[6,64,8,64]{3,2,1,0:T(8,128)(2,1)S(1)} %reshape.83) | copy-start | bytes 1179652
  62.7 0.7 copy-start.1
  63.3 106.3 %reduce-scatter.2.cloned.1.call-start = ((), (), s32[]{:S(2)}) async-start(), calls=%async_computation.2 | async-start | bytes 2359296 | tf_op jit(solution)/shard_map/reduce_scatter | solution.py:148
  63.4 3.3 %copy-start.7 = (bf16[384,2048]{1,0:T(8,128)(2,1)S(1)}, bf16[384,2048]{1,0:T(8,128)(2,1)}, u32[]{:S(2)}) copy-start(bf16[384,2048]{1,0:T(8,128)(2,1)} %all-gather.5.cloned.1.call-done) | copy-start | bytes 4718596
  63.4 3.3 %copy-start.11 = (bf16[2048,512]{1,0:T(8,128)(2,1)S(1)}, bf16[2048,512]{1,0:T(8,128)(2,1)}, u32[]{:S(2)}) copy-start(bf16[2048,512]{1,0:T(8,128)(2,1)} %param.25) | copy-start | bytes 6291460
  67.7 3.8 %copy-start.10 = (bf16[384,512]{1,0:T(8,128)(2,1)}, bf16[384,512]{1,0:T(8,128)(2,1)S(1)}, u32[]{:S(2)}) copy-start(bf16[384,512]{1,0:T(8,128)(2,1)S(1)} %fusion.12) | copy-start | bytes 1179652
  67.7 52.9 %collective-permute-start = (bf16[2,512]{1,0:T(2,128)(2,1)S(1)}, bf16[2,512]{1,0:T(2,128)(2,1)S(1)}, u32[]{:S(2)}, u32[]{:S(2)}) collective-permute-start(bf16[2,512]{1,0:T(2,128)(2,1)S(1)} %slice.28), channel_id=1, source_target_pairs={{0,2},{2,4},{4,6},{6,8},{8,10},{10,12},{12,14},{14,16},{16,18},{18... | collective-permute-start | bytes 6152 | tf_op jit(solution)/shard_map/ppermute | solution.py:16
  74.5 4.4 %copy-start.3 = (bf16[6,64,8,64]{3,2,1,0:T(8,128)(2,1)S(1)}, bf16[6,64,8,64]{3,2,1,0:T(8,128)(2,1)}, u32[]{:S(2)}) copy-start(bf16[6,64,8,64]{3,2,1,0:T(8,128)(2,1)} %copy-done.2) | copy-start | bytes 1179652
  126.8 0.9 copy-start.9
  137.9 2.6 %copy-start.8 = (f32[384,512]{1,0:T(8,128)S(1)}, f32[384,512]{1,0:T(8,128)}, u32[]{:S(2)}) copy-start(f32[384,512]{1,0:T(8,128)} %copy.66) | copy-start | bytes 2359300
Sparse Core Ops, SparseCore 0:
  8.9 12.5 all-gather.4
  63.5 61.8 all-gather.6
  147.7 21.8 reduce-scatter.1
where the time goes:
time: 177 us; the launch traced here: 176 us
  matrix products  42 us (24%)
  blocking collectives  39.2 us (22%)
  waiting for transfers between devices  34.5 us (19%)
  local copies, waits for them, and re-layouts  21.5 us (12%)
  other arithmetic  21.3 us (12%)
  between operations  13.4 us (8%)
  starting transfers between devices  3.88 us (2%)
    all_gather x1, blocking collectives, prefix(): gathered = jax.tree.map(lambda a: lax.all_gather(a, axis), part)  39.2 us
    reduce_scatter x1, waiting for transfers between devices, on_device(): lax.psum_scatter((jnp.dot(conv_out, convolution_output_weight, preferred_...  22 us
    dot_general x6, matrix products, on_device(): jnp.dot(normed, weight, preferred_element_type=jnp.float32)  13.9 us
    all_gather x1, waiting for transfers between devices, on_device(): lax.all_gather(tokens, 'tp', axis=1, tiled=True).astype(jnp.float32)  11.8 us
    dot_general x1, matrix products, on_device(): jnp.dot(attn_out, attention_output_weight, preferred_element_type=jnp.flo...  7.02 us
    add x6, other arithmetic, carry_step(): return (block_decay[..., None] * state + update, state)  6.13 us
    dot_general x1, matrix products, on_device(): jnp.dot(conv_out, convolution_output_weight, preferred_element_type=jnp.f...  6.1 us
    dot_general x1, matrix products, on_device(): jnp.einsum('nchd,nhde->nche', query_g, entering, precision=lax.Precision....  5.72 us
  transfers between devices with their start and end apart: 4, of which 2 were waited for; matrix products, arithmetic and copies ran while one was open for 13% of the time, Pallas kernels for 0%

commit v1 on v0

v1 whole, which is shorter than its diff:
```python
import functools

import jax
import jax.numpy as jnp
from jax import lax
from jax.experimental import pallas as pl
from jax.experimental.pallas import tpu as pltpu
from jax.sharding import PartitionSpec as P

BLOCK = 64
NORM_EPS = 1e-06
GATE_SOFTNESS = 16.0
F32 = jnp.float32
BF16 = jnp.bfloat16
NT = (((1,), (1,)), ((), ()))
TN = (((0,), (0,)), ((), ()))
VMEM = pl.BlockSpec(memory_space=pltpu.VMEM)
SMEM = pl.BlockSpec(memory_space=pltpu.SMEM)
HBM = pl.BlockSpec(memory_space=pl.ANY)
EXTRA_ROWS = 16


def dot(a, b):
    return jnp.dot(a, b, preferred_element_type=F32)


def call(body, outs, ins, flops, scratch=(), limit=48 << 20, name=None):
    specs = [s for _, s in ins]
    return pl.pallas_call(
        body,
        out_shape=[jax.ShapeDtypeStruct(s, d) for s, d in outs],
        in_specs=specs,
        out_specs=[VMEM] * len(outs),
        scratch_shapes=list(scratch),
        compiler_params=pltpu.CompilerParams(vmem_limit_bytes=limit),
        cost_estimate=pl.CostEstimate(flops=flops, bytes_accessed=1 << 20, transcendentals=0),
        name=name,
    )(*[a for a, _ in ins])


def weight_copies(hbm, buf, sems, row, rows):
    copies, at = [], 0
    for i, w in enumerate(hbm):
        cols = w.shape[1]
        copies.append(
            pltpu.make_async_copy(
                w.at[pl.ds(row, rows), :], buf.at[:, at : at + cols], sems.at[i]
            )
        )
        at += cols
    return copies


def tile_lanes(column, lanes):
    return jnp.concatenate([column] * (lanes // column.shape[1]), axis=1)


def block_mask(rows, row_step, lanes, lane_step):
    r = lax.broadcasted_iota(jnp.int32, (rows, lanes), 0) // row_step
    c = lax.broadcasted_iota(jnp.int32, (rows, lanes), 1) // lane_step
    return r == c


def own_half(tp, tok, gain, extra, *refs):
    weights, (acc, xg, ssq, wide), (buf, sems) = refs[:5], refs[5:9], refs[9:]
    half = tok.shape[1]
    at = pl.multiple_of(tp[0] * half, half)
    copies = weight_copies(weights, buf, sems, at, half)
    for c in copies:
        c.start()
    x = tok[...].astype(F32)
    ssq[...] = jnp.broadcast_to(jnp.sum(x * x, axis=1, keepdims=True), ssq.shape)
    xg[...] = (x * gain[:, pl.ds(at, half)]).astype(BF16)
    heads = extra.shape[1]
    lanes = wide.shape[1]
    r = lax.broadcasted_iota(jnp.int32, (heads, lanes), 0)
    c = lax.broadcasted_iota(jnp.int32, (heads, lanes), 1) // (lanes // heads)
    wide[...] = jnp.dot(
        extra[...],
        (r == c).astype(F32),
        precision=lax.Precision.HIGHEST,
        preferred_element_type=F32,
    )
    left = xg[...]
    at = 0
    for c, w in zip(copies, weights):
        cols = w.shape[1]
        c.wait()
        acc[:, at : at + cols] = dot(left, buf[:, at : at + cols])
        at += cols


def other_half(tp, tok, gain, bias, acc, xg, ssq, wide, *refs):
    weights = refs[:5]
    full, scale, key, val, cum, base, prod, own, send = refs[5:14]
    buf, sems = refs[14:]
    rows, half = tok.shape
    at = pl.multiple_of((1 - tp[0]) * half, half)
    copies = weight_copies(weights, buf, sems, at, half)
    for c in copies:
        c.start()
    x = tok[...].astype(F32)
    power = (ssq[:, :1] + jnp.sum(x * x, axis=1, keepdims=True)) * (0.5 / half)
    r = jnp.broadcast_to(lax.rsqrt(power + NORM_EPS), scale.shape)
    scale[...] = r
    left = (x * gain[:, pl.ds(at, half)]).astype(BF16)
    full[:, pl.ds(at, half)] = left
    full[:, pl.ds(pl.multiple_of(tp[0] * half, half), half)] = xg[...]

    def project(i, lo, hi):
        copies[i].wait()
        s = acc[:, lo:hi] + dot(left, buf[:, lo:hi])
        return (s * tile_lanes(r, hi - lo)).astype(BF16)

    kw = weights[0].shape[1]
    vw = weights[2].shape[1]
    cw = weights[3].shape[1]
    k = project(0, 0, kw)
    key[...] = k
    f = project(1, kw, 2 * kw).astype(F32) + bias[...]
    log = (jnp.minimum(f, 0.0) - jnp.log1p(jnp.exp(-jnp.abs(f)))) * (1.0 / GATE_SOFTNESS)
    log = log + wide[...]
    hi = log.astype(BF16)
    rest = log - hi.astype(F32)
    mid = rest.astype(BF16)
    low = (rest - mid.astype(F32)).astype(BF16)
    tri = (
        lax.broadcasted_iota(jnp.int32, (BLOCK, 3 * BLOCK), 0)
        >= lax.broadcasted_iota(jnp.int32, (BLOCK, 3 * BLOCK), 1) % BLOCK
    ).astype(BF16)
    n = rows // BLOCK
    running = jnp.zeros((1, kw), F32)
    starts = []
    for b in range(n):
        s = slice(b * BLOCK, (b + 1) * BLOCK)
        part = dot(tri, jnp.concatenate([hi[s], mid[s], low[s]], axis=0))
        cum[s, :] = part
        starts.append(running)
        running = running + part[BLOCK - 1 :]
    base[...] = jnp.concatenate(starts + [running] * (base.shape[0] - n), axis=0)
    kf = k.astype(F32)
    decayed = []
    for b in range(n):
        s = slice(b * BLOCK, (b + 1) * BLOCK)
        decayed.append((kf[s] * jnp.exp((running - starts[b]) - cum[s, :])).astype(BF16))
    decayed = jnp.concatenate(decayed, axis=0)
    val[...] = project(2, 2 * kw, 2 * kw + vw)
    dv = own.shape[0]
    group = vw // 256
    for g in range(group):
        m = lax.dot_general(
            val[:, g * 256 : (g + 1) * 256],
            decayed[:, g * 128 : (g + 1) * 128],
            TN,
            preferred_element_type=F32,
        )
        own[:, g * 128 : (g + 1) * 128] = fold(m, dv)
    at = 2 * kw + vw
    c_in = project(3, at, at + cw).astype(F32)
    h_in = project(4, at + cw, at + 2 * cw).astype(F32)
    p = c_in * h_in
    p = p.astype(BF16)
    prod[...] = p
    last = p[rows - 16 :].astype(F32)
    pack(send, own[...], jnp.exp(running), [last[14:15, :kw], last[14:15, kw:], last[15:, :kw], last[15:, kw:]])


def fold(m, dv):
    step = m.shape[1] // (m.shape[0] // dv)
    lane = lax.broadcasted_iota(jnp.int32, (dv, m.shape[1]), 1) // step
    out = m[:dv]
    for h in range(1, m.shape[0] // dv):
        out = jnp.where(lane == h, m[h * dv : (h + 1) * dv], out)
    return out


def pack(ref, state, decay, halo):
    dv = state.shape[0]
    ref[:dv, :] = state.astype(BF16)
    top = decay.astype(BF16).astype(F32)
    row = lax.broadcasted_iota(jnp.int32, (EXTRA_ROWS, state.shape[1]), 0)
    tail = jnp.zeros((EXTRA_ROWS, state.shape[1]), F32)
    for i, v in enumerate([top, decay - top] + list(halo)):
        tail = jnp.where(row == i, v, tail)
    ref[dv:, :] = tail.astype(BF16)


def unpack(v, dv):
    tail = v[dv:].astype(F32)
    return v[:dv].astype(F32), tail[0:1] + tail[1:2], tail


def fold_round(digit, low_zero, stack, radix, dv):
    lanes = stack.shape[2]
    pre_s, pre_d = jnp.zeros((dv, lanes), F32), jnp.ones((1, lanes), F32)
    tot_s, tot_d = pre_s, pre_d
    halo = jnp.zeros((EXTRA_ROWS, lanes), F32)
    for j in range(radix):
        s, d, tail = unpack(stack[j ^ digit], dv)
        before = j < digit
        pre_s = jnp.where(before, d * pre_s + s, pre_s)
        pre_d = jnp.where(before, d * pre_d, pre_d)
        halo = jnp.where((j + 1 == digit) & (low_zero > 0), tail, halo)
        tot_s, tot_d = d * tot_s + s, d * tot_d
    return pre_s, pre_d, tot_s, tot_d, tail, halo


def join_round(radix, place, *refs):
    items, (sp, dp, hp), (send, s_out, d_out, h_out), (stack,) = (
        refs[:radix],
        refs[radix : radix + 3],
        refs[radix + 3 : radix + 7],
        refs[radix + 7 :],
    )
    dv = sp.shape[0]
    for i, item in enumerate(items):
        stack[i] = item[...]
    pre_s, pre_d, tot_s, tot_d, tail, halo = fold_round(place[0], place[1], stack, radix, dv)
    s_out[...] = dp[0:1] * pre_s + sp[...]
    d_out[...] = jnp.broadcast_to(dp[0:1] * pre_d, d_out.shape)
    h_out[...] = halo + hp[...]
    pack(send, tot_s, tot_d, [tail[2:3], tail[3:4], tail[4:5], tail[5:6]])


def late_half(full, scale, prod, taps, gain, wq, wb, wg, query, outer, gate, conv):
    r = scale[...]
    x = full[...]

    def project(w):
        s = dot(x, w[...])
        return (s * tile_lanes(r, s.shape[1])).astype(BF16)

    b = project(wb)
    outer[...] = b
    p = prod[...].astype(F32)
    rows = p.shape[0]
    row = lax.broadcasted_iota(jnp.int32, p.shape, 0)
    t = taps[...].astype(F32)
    total = jnp.zeros(p.shape, F32)
    for j in range(taps.shape[0] - 1):
        back = taps.shape[0] - 1 - j
        total = total + t[j : j + 1] * jnp.where(row >= back, pltpu.roll(p, back, 0), 0.0)
    total = total + t[taps.shape[0] - 1 :] * p
    conv[...] = (b.astype(F32) * total).astype(BF16)
    query[...] = project(wq)
    g = project(wg).astype(F32)
    gate[...] = g * jax.nn.sigmoid(g) * gain[...]


def blockwise(key_dim, query, key, val, cum, base, start, raw, through, first):
    rows = query.shape[0]
    n = rows // BLOCK
    scale = key_dim**-0.5
    first[...] = start[...].T
    k_mask = block_mask(256, 64, 128, 32)
    v_mask = block_mask(256, 64, 256, 64)
    causal = lax.broadcasted_iota(jnp.int32, (BLOCK, 256), 0) >= (
        lax.broadcasted_iota(jnp.int32, (BLOCK, 256), 1) % BLOCK
    )
    zero = jnp.zeros((), BF16)
    for g in range(val.shape[1] // 256):
        kl = slice(g * 128, (g + 1) * 128)
        vl = slice(g * 256, (g + 1) * 256)
        state = None
        for b in range(n):
            s = slice(b * BLOCK, (b + 1) * BLOCK)
            c = cum[s, kl]
            q = query[s, kl].astype(F32) * scale
            k = key[s, kl].astype(F32)
            end = c[BLOCK - 1 :]
            q_in = (q * jnp.exp(c)).astype(BF16)
            k_in = (k * jnp.exp(-c)).astype(BF16)
            through[s, kl] = (q * jnp.exp(c + base[b : b + 1, kl])).astype(BF16)
            v = val[s, vl]
            k_wide = jnp.where(k_mask, jnp.concatenate([k_in] * 4, axis=0), zero)
            scores = lax.dot_general(q_in, k_wide, NT, preferred_element_type=F32)
            scores = jnp.where(causal, scores, 0.0).astype(BF16)
            v_wide = jnp.where(v_mask, jnp.concatenate([v] * 4, axis=0), zero)
            out = dot(scores, v_wide)
            if state is not None:
                out = out + lax.dot_general(
                    q_in, state.astype(BF16), NT, preferred_element_type=F32
                )
            raw[s, vl] = out
            if b < n - 1:
                k_out = (k * jnp.exp(end - c)).astype(BF16)
                new = lax.dot_general(v, k_out, TN, preferred_element_type=F32)
                new = jnp.where(k_mask, new, 0.0)
                state = new if state is None else state * jnp.exp(end) + new


def rows_out(half, incoming, halo, raw, through, gate, conv, outer, prod, taps, wc, wa):
    rows = raw.shape[0] // 2
    at = pl.multiple_of(half * rows, 64)
    here = pl.ds(at, rows)
    ones = block_mask(256, 64, 256, 64).astype(BF16) * (1.0 / 64)
    ones = ones.astype(BF16)
    parts = []
    for g in range(raw.shape[1] // 256):
        vl = slice(g * 256, (g + 1) * 256)
        x = raw[here, vl] + lax.dot_general(
            through[here, g * 128 : (g + 1) * 128],
            incoming[g],
            NT,
            preferred_element_type=F32,
        )
        mean = dot((x * x).astype(BF16), ones)
        parts.append((x * lax.rsqrt(mean + NORM_EPS) * gate[here, vl]).astype(BF16))
    attn = jnp.concatenate(parts, axis=1)
    p = prod[:16, :].astype(F32)
    wide = p.shape[1]
    row = lax.broadcasted_iota(jnp.int32, p.shape, 0)
    t = taps[...].astype(F32)
    back2 = jnp.where(row == 0, halo[0:1], jnp.where(row == 1, halo[1:2], pltpu.roll(p, 2, 0)))
    back1 = jnp.where(row == 0, halo[1:2], pltpu.roll(p, 1, 0))
    top = outer[:16, :].astype(F32) * (t[0:1] * back2 + t[1:2] * back1 + t[2:3] * p)
    mine = conv[here, :]
    head = jnp.where(half == 0, top, mine[:16].astype(F32)).astype(BF16)
    left = jnp.concatenate([head, mine[16:]], axis=0)
    return left, attn


def project_out(left, attn, wc, wa, out):
    step = 512
    for n in range(0, out.shape[1], step):
        s = dot(left, wc[:, n : n + step]) + dot(attn, wa[:, n : n + step])
        out[:, n : n + step] = s.astype(out.dtype)


def partner_rows(radix, place, *refs):
    items = refs[:radix]
    sp, dp, hp, first, raw, through, gate, conv, outer, prod, taps, wc, wa = refs[radix : radix + 13]
    out, state, halo_out, stack = refs[radix + 13 :]
    dv = sp.shape[0]
    for i, item in enumerate(items):
        stack[i] = item[...]
    digit, low_zero, half = place[0], place[1], 1 - place[2]
    lanes = stack.shape[2]
    pre_s = first[...]
    halo = hp[...]
    for j in range(radix):
        s, d, tail = unpack(stack[j ^ digit], dv)
        pre_s = jnp.where(j < digit, d * pre_s + s, pre_s)
        halo = jnp.where((j + 1 == digit) & (low_zero > 0), tail, halo)
    pre_s = dp[0:1] * pre_s + sp[...]
    mask = block_mask(256, 64, 128, 32)
    incoming = []
    for g in range(lanes // 128):
        s = pre_s[:, g * 128 : (g + 1) * 128]
        wide = jnp.where(mask, jnp.concatenate([s] * 4, axis=0), 0.0).astype(BF16)
        incoming.append(wide)
        state[g] = wide
    rows2 = jnp.concatenate(
        [jnp.concatenate([halo[2:3], halo[3:4]], axis=1), jnp.concatenate([halo[4:5], halo[5:6]], axis=1)],
        axis=0,
    )
    halo_out[...] = jnp.concatenate([rows2] * 4, axis=0)
    left, attn = rows_out(half, incoming, rows2, raw, through, gate, conv, outer, prod, taps, wc, wa)
    project_out(left, attn, wc, wa, out)


def own_rows(place, state, halo, raw, through, gate, conv, outer, prod, taps, wc, wa, out):
    incoming = [state[g] for g in range(state.shape[0])]
    left, attn = rows_out(
        place[2], incoming, halo[0:2, :], raw, through, gate, conv, outer, prod, taps, wc, wa
    )
    project_out(left, attn, wc, wa, out)


def add_rows(a, b, out):
    out[...] = (a[...] + b[...].astype(F32)).astype(BF16)


def radices(n):
    found = []
    while n > 1:
        r = 4 if n % 4 == 0 else 2
        found.append(r)
        n //= r
    return found


def on_device(
    tokens,
    input_norm_gain,
    outer_gate_weight,
    inner_gate_weight,
    convolution_input_weight,
    convolution_kernel_taps,
    query_weight_matrix,
    key_weight_matrix,
    value_weight_matrix,
    forget_gate_weight,
    attention_gate_weight,
    forget_gate_bias,
    extra_logarithm_decay,
    initial_head_state,
    head_norm_gain,
    convolution_output_weight,
    attention_output_weight,
):
    rows, half = tokens.shape
    heads, dk, dv = initial_head_state.shape
    kw, vw, cw = heads * dk, heads * dv, outer_gate_weight.shape[1]
    model = convolution_output_weight.shape[1]
    n_sp = lax.axis_size("sp")
    tp = lax.axis_index("tp").astype(jnp.int32)
    sp = lax.axis_index("sp").astype(jnp.int32)
    swap = [(0, 1), (1, 0)]
    other = lax.ppermute(tokens, "tp", swap)
    gain = input_norm_gain.reshape(1, -1)
    tp1 = tp.reshape(1)
    early = (
        key_weight_matrix,
        forget_gate_weight,
        value_weight_matrix,
        inner_gate_weight,
        convolution_input_weight,
    )
    width = sum(w.shape[1] for w in early)
    buffers = [pltpu.VMEM((half, width), BF16), pltpu.SemaphoreType.DMA((5,))]
    flops = 2 * rows * half * width
    acc, xg, ssq, wide = call(
        own_half,
        [((rows, width), F32), ((rows, half), BF16), ((rows, 128), F32), ((rows, kw), F32)],
        [(tp1, SMEM), (tokens, VMEM), (gain, VMEM), (extra_logarithm_decay, VMEM)]
        + [(w, HBM) for w in early],
        flops,
        buffers,
        name="own_half",
    )
    full, scale, key, val, cum, base, prod, own, send = call(
        other_half,
        [
            ((rows, 2 * half), BF16),
            ((rows, 128), F32),
            ((rows, kw), BF16),
            ((rows, vw), BF16),
            ((rows, kw), F32),
            ((8, kw), F32),
            ((rows, cw), BF16),
            ((dv, kw), F32),
            ((dv + EXTRA_ROWS, kw), BF16),
        ],
        [(tp1, SMEM), (other, VMEM), (gain, VMEM), (forget_gate_bias.reshape(1, -1), VMEM)]
        + [(a, VMEM) for a in (acc, xg, ssq, wide)]
        + [(w, HBM) for w in early],
        flops,
        buffers,
        name="other_half",
    )
    query, outer, gate, conv = call(
        late_half,
        [((rows, kw), BF16), ((rows, cw), BF16), ((rows, vw), F32), ((rows, cw), BF16)],
        [
            (full, VMEM),
            (scale, VMEM),
            (prod, VMEM),
            (convolution_kernel_taps, VMEM),
            (jnp.tile(head_norm_gain.reshape(1, -1), (1, heads)), VMEM),
            (query_weight_matrix, VMEM),
            (outer_gate_weight, VMEM),
            (attention_gate_weight, VMEM),
        ],
        2 * rows * 2 * half * (kw + vw + cw),
        name="late_half",
    )
    raw, through, first = call(
        functools.partial(blockwise, dk),
        [((rows, vw), F32), ((rows, kw), BF16), ((dv, kw), F32)],
        [
            (a, VMEM)
            for a in (query, key, val, cum, base, initial_head_state.reshape(heads * dk, dv))
        ],
        2 * rows * 2 * half * (kw + vw),
        name="blockwise",
    )
    pre = (
        jnp.zeros((dv, kw), F32),
        jnp.ones((8, kw), F32),
        jnp.zeros((EXTRA_ROWS, kw), F32),
    )
    stride = 1
    plan = radices(n_sp)
    for turn, radix in enumerate(plan):
        items = [send]
        for j in range(1, radix):
            items.append(lax.ppermute(send, "sp", [(i, i ^ (j * stride)) for i in range(n_sp)]))
        digit = (sp // stride) % radix
        low_zero = (sp % stride == 0).astype(jnp.int32)
        place = jnp.stack([digit, low_zero, tp])
        stack = [pltpu.VMEM((radix,) + send.shape, BF16)]
        if turn < len(plan) - 1:
            send, *pre = call(
                functools.partial(join_round, radix),
                [(send.shape, BF16), ((dv, kw), F32), ((8, kw), F32), ((EXTRA_ROWS, kw), F32)],
                [(place, SMEM)] + [(a, VMEM) for a in items] + [(a, VMEM) for a in pre],
                1 << 20,
                stack,
                name="join_round",
            )
        stride *= radix
    tail = [
        (a, VMEM)
        for a in (
            raw,
            through,
            gate,
            conv,
            outer,
            prod,
            convolution_kernel_taps,
            convolution_output_weight,
            attention_output_weight,
        )
    ]
    flops = 2 * (rows // 2) * model * (vw + cw)
    theirs, state, halo = call(
        functools.partial(partner_rows, plan[-1]),
        [((rows // 2, model), BF16), ((kw // 128, 256, 128), BF16), ((8, cw), F32)],
        [(place, SMEM)] + [(a, VMEM) for a in items] + [(a, VMEM) for a in (*pre, first)] + tail,
        flops,
        stack,
        name="partner_rows",
    )
    got = lax.ppermute(theirs, "tp", swap)
    (mine,) = call(
        own_rows,
        [((rows // 2, model), F32)],
        [(place, SMEM), (state, VMEM), (halo, VMEM)] + tail,
        flops,
        name="own_rows",
    )
    return (mine + got.astype(F32)).astype(BF16)


def solution(mesh):
    placed = (
        P("sp", "tp"),
        P(),
        P(None, "tp"),
        P(None, "tp"),
        P(None, "tp"),
        P(None, "tp"),
        P(None, "tp"),
        P(None, "tp"),
        P(None, "tp"),
        P(None, "tp"),
        P(None, "tp"),
        P("tp"),
        P("sp", "tp"),
        P("tp", None, None),
        P(),
        P("tp", None),
        P("tp", None),
    )
    return jax.shard_map(
        on_device, mesh=mesh, in_specs=placed, out_specs=P(("sp", "tp"), None), check_vma=False
    )
```

time: 177 us -> 48.9 us (0.28)
  matrix products: 42 us -> 0 us
  blocking collectives: 39.2 us -> 0 us
  waiting for transfers between devices: 34.5 us -> 4.27 us
  Pallas kernels: 0 us -> 26.2 us
  other arithmetic: 21.3 us -> 1.25 us
  local copies, waits for them, and re-layouts: 21.5 us -> 7.3 us
  between operations: 13.4 us -> 0.19 us
  starting transfers between devices: 3.88 us -> 9.34 us
    dot_general x12 -> x0, matrix products: 42 us -> none  [the longest x6 13.9 us: on_device(): jnp.dot(normed, weight, preferred_element_type=jnp.float32)]
    all_gather x1 -> x0, blocking collectives: 39.2 us -> none  [prefix(): gathered = jax.tree.map(lambda a: lax.all_gather(a, axis), part)]
    pallas_call x0 -> x7, Pallas kernels: none -> 26.2 us  [call(): pl.pallas_call(body, out_shape=[jax.ShapeDtypeStruct(s, d) for s, d in ou...]
    reduce_scatter x1 -> x0, waiting for transfers between devices: 22 us -> none  [on_device(): lax.psum_scatter((jnp.dot(conv_out, convolution_output_weight, preferred_...]
    all_gather x2 -> x0, waiting for transfers between devices: 11.8 us -> none  [the longest x1 11.8 us: on_device(): lax.all_gather(tokens, 'tp', axis=1, tiled=True).astype(jnp.float32)]
    reshape x5 -> x0, local copies, waits for them, and re-layouts: 7.32 us -> none  [the longest x1 2.65 us: on_device(): raw = (inner + outer).reshape(number_of_rows, number_of_heads, value_dim)]
    add x8 -> x0, other arithmetic: 7.29 us -> none  [the longest x6 6.13 us: carry_step(): return (block_decay[..., None] * state + update, state)]
    add x3 -> x0, local copies, waits for them, and re-layouts: 6.7 us -> none  [the longest x2 3.66 us: on_device(): logarithm_decay.reshape(number_of_rows, number_of_heads, key_channel_count)]
  transfers between devices with their start and end apart: 4 -> 8, of which waited for: 2 -> 2; matrix products, arithmetic and copies ran while one was open for 13% -> 4% of each run, Pallas kernels for 0% -> 31%
where the time goes in v1:
time: 48.9 us; the launch traced here: 48.5 us
  Pallas kernels  26.2 us (54%)
  starting transfers between devices  9.34 us (19%)
  local copies, waits for them, and re-layouts  7.3 us (15%)
  waiting for transfers between devices  4.27 us (9%)
  other arithmetic  1.25 us (3%)
    pallas_call x7, Pallas kernels, call(): pl.pallas_call(body, out_shape=[jax.ShapeDtypeStruct(s, d) for s, d in ou...  26.2 us
    ppermute x6, starting transfers between devices, on_device(): lax.ppermute(send, 'sp', [(i, i ^ j * stride) for i in range(n_sp)])  8.77 us
    unnamed x23, local copies, waits for them, and re-layouts  6.54 us
    ppermute x6, waiting for transfers between devices, on_device(): lax.ppermute(send, 'sp', [(i, i ^ j * stride) for i in range(n_sp)])  4.26 us
    convert_element_type x1, other arithmetic, on_device(): return (mine + got.astype(F32)).astype(BF16)  1.1 us
  transfers between devices with their start and end apart: 8, of which 2 were waited for; matrix products, arithmetic and copies ran while one was open for 4% of the time, Pallas kernels for 31%

profile of v1, /device:TPU:0, one launch (start us, length us, event | category | flops | bytes accessed | tf_op | source)
XLA Modules:
  0.0 48.5 jit_solution(1840612502144069993)
XLA Ops:
  0.0 0.5 %collective-permute-start = (bf16[384,1024]{1,0:T(8,128)(2,1)}, bf16[384,1024]{1,0:T(8,128)(2,1)S(1)}, u32[]{:S(2)}, u32[]{:S(2)}) collective-permute-start(bf16[384,1024]{1,0:T(8,128)(2,1)} %tok.1), channel_id=1, source_target_pairs={{0,1},{1,0},{2,3},{3,2},{4,5},{5,4},{6,7},{7,6},{8,9},{9,8},{10,11... | collective-permute-start | bytes 2359304 | tf_op jit(solution)/shard_map/ppermute | solution.py:410
  0.5 0.8 %copy.18.extra = f32[384,8]{1,0:T(8,128)S(1)} copy(f32[384,8]{0,1:T(8,128)} %param.29) | data formatting | bytes 24576 | tf_op args[12]
  1.3 0.7 %tile.8 = f32[8,64]{1,0:T(8,128)S(1)} broadcast(f32[64]{0:T(128)} %param.31), dimensions={1} | broadcast | bytes 2304 | tf_op jit(solution)/shard_map/tile | solution.py:460
  2.0 0.1 tile.9.gain
  2.1 0.1 add_add_fusion.1.place
  2.1 0.1 add_add_fusion.place
  2.2 0.0 copy-start
  2.2 1.2 %copy-done = bf16[2048,256]{1,0:T(8,128)(2,1)S(1)} copy-done((bf16[2048,256]{1,0:T(8,128)(2,1)S(1)}, bf16[2048,256]{1,0:T(8,128)(2,1)}, u32[]{:S(2)}) %copy-start) | copy-done | bytes 1048600
  3.4 0.0 copy-start.2
  3.5 1.2 %copy-done.2 = bf16[2048,256]{1,0:T(8,128)(2,1)S(1)} copy-done((bf16[2048,256]{1,0:T(8,128)(2,1)S(1)}, bf16[2048,256]{1,0:T(8,128)(2,1)}, u32[]{:S(2)}) %copy-start.2) | copy-done | bytes 1048600
  4.7 0.0 copy-start.4
  4.7 1.1 %copy-done.4 = bf16[384,1024]{1,0:T(8,128)(2,1)S(1)} copy-done((bf16[384,1024]{1,0:T(8,128)(2,1)S(1)}, bf16[384,1024]{1,0:T(8,128)(2,1)}, u32[]{:S(2)}) %copy-start.4) | copy-done | bytes 786456
  5.8 0.0 copy-start.5
  5.8 0.7 %copy-done.5 = f32[2048]{0:T(1024)S(1)} copy-done((f32[2048]{0:T(1024)S(1)}, f32[2048]{0:T(1024)}, u32[]{:S(2)}) %copy-start.5) | copy-done | bytes 8216
  6.5 0.0 copy-start.1
  6.5 0.0 copy-start.3
  6.5 5.5 %own_half.1 = (f32[384,2048]{1,0:T(8,128)}, bf16[384,1024]{1,0:T(8,128)(2,1)S(1)}, f32[384,128]{1,0:T(8,128)S(1)}, f32[384,256]{1,0:T(8,128)S(1)}) custom-call(s32[1]{0:T(128)} %bitcast.2.tp, bf16[384,1024]{1,0:T(8,128)(2,1)S(1)} %copy-done.4, f32[1,2048]{1,0:T(1,128)S(1)} %bitcast.7, f32[384,8]{1,0:T(8,128)S(1)} %copy.18.extra, ...), custom_call_target="tpu_custom_call" | custom-call | flops 1610612736 | bytes 1048576 | tf_op jit(solution)/shard_map/own_half/pallas_call | solution.py:29
  12.1 0.0 collective-permute-done.tok
  12.1 0.0 copy-done.1
  12.1 0.0 copy-done.3
  12.1 0.0 copy-done.7
  12.1 0.0 copy-start.6
  12.1 0.0 copy-start.9
  12.1 6.9 %other_half.1 = (bf16[384,2048]{1,0:T(8,128)(2,1)}, f32[384,128]{1,0:T(8,128)S(1)}, bf16[384,256]{1,0:T(8,128)(2,1)S(1)}, bf16[384,512]{1,0:T(8,128)(2,1)S(1)}, ...) custom-call(s32[1]{0:T(128)} %bitcast.2.tp, ...), custom_call_target="tpu_custom_call" | custom-call | flops 1610612736 | bytes 1048576 | tf_op jit(solution)/shard_map/other_half/pallas_call | solution.py:29
  19.0 2.5 %collective-permute-start.1 = (bf16[80,256]{1,0:T(8,128)(2,1)S(1)}, bf16[80,256]{1,0:T(8,128)(2,1)S(1)}, u32[]{:S(2)}, u32[]{:S(2)}) collective-permute-start(bf16[80,256]{1,0:T(8,128)(2,1)S(1)} %get-tuple-element.35.refs_0_), channel_id=1, source_target_pairs={{0,2},{2,0},{4,6},{6,4},{8,10},{10,8},{12,14},{14,12},{16,18},{18,... | collective-permute-start | bytes 122888 | tf_op jit(solution)/shard_map/ppermute | solution.py:488
  21.6 1.5 %collective-permute-start.2 = (bf16[80,256]{1,0:T(8,128)(2,1)S(1)}, bf16[80,256]{1,0:T(8,128)(2,1)S(1)}, u32[]{:S(2)}, u32[]{:S(2)}) collective-permute-start(bf16[80,256]{1,0:T(8,128)(2,1)S(1)} %get-tuple-element.35.refs_0_), channel_id=1, source_target_pairs={{0,4},{2,6},{4,0},{6,2},{8,12},{10,14},{12,8},{14,10},{16,20},{18,... | collective-permute-start | bytes 122888 | tf_op jit(solution)/shard_map/ppermute | solution.py:488
  23.1 0.0 collective-permute-start.3
  23.1 0.0 copy-done.6
  23.1 0.0 copy-done.9
  23.1 1.4 %copy-done.8 = bf16[384,2048]{1,0:T(8,128)(2,1)S(1)} copy-done((bf16[384,2048]{1,0:T(8,128)(2,1)S(1)}, bf16[384,2048]{1,0:T(8,128)(2,1)}, u32[]{:S(2)}) %copy-start.8) | copy-done | bytes 1572888
  24.5 4.6 %late_half.1 = (bf16[384,256]{1,0:T(8,128)(2,1)S(1)}, bf16[384,512]{1,0:T(8,128)(2,1)S(1)}, f32[384,512]{1,0:T(8,128)S(1)}, bf16[384,512]{1,0:T(8,128)(2,1)S(1)}) custom-call(bf16[384,2048]{1,0:T(8,128)(2,1)S(1)} %copy-done.8, f32[384,128]{1,0:T(8,128)S(1)} %get-tuple-element.41.scale, bf16[384,512]{1,0:T(8,128)(2,1)S(1)} %get-tuple-element.42.prod.refs_13_, ...), custom_call_target="tpu_custom_call" | custom-call | flops 2013265920 | bytes 1048576 | tf_op jit(solution)/shard_map/late_half/pallas_call | solution.py:29
  29.1 0.0 collective-permute-done.1.refs_1_
  29.1 0.0 collective-permute-done.2.refs_2_
  29.1 0.0 collective-permute-done.3.refs_3_
  29.2 0.6 %join_round.1 = (bf16[80,256]{1,0:T(8,128)(2,1)S(1)}, f32[64,256]{1,0:T(8,128)S(1)}, f32[8,256]{1,0:T(8,128)S(1)}, f32[16,256]{1,0:T(8,128)S(1)}) custom-call(s32[3]{0:T(128)S(1)} %add_add_fusion.1.place, bf16[80,256]{1,0:T(8,128)(2,1)S(1)} %get-tuple-element.35.refs_0_, bf16[80,256]{1,0:T(8,128)(2,1)S(1)} %collective-permute-done.1.refs_1_, ...), custom_call_target="tpu_custom_call" | custom-call | flops 1048576 | bytes 1048576 | tf_op jit(solution)/shard_map/join_round/pallas_call | solution.py:29
  29.8 2.1 %collective-permute-start.4 = (bf16[80,256]{1,0:T(8,128)(2,1)S(1)}, bf16[80,256]{1,0:T(8,128)(2,1)S(1)}, u32[]{:S(2)}, u32[]{:S(2)}) collective-permute-start(bf16[80,256]{1,0:T(8,128)(2,1)S(1)} %get-tuple-element.36.refs_0_), channel_id=1, source_target_pairs={{0,8},{2,10},{4,12},{6,14},{8,0},{10,2},{12,4},{14,6},{16,24},{18,... | collective-permute-start | bytes 122888 | tf_op jit(solution)/shard_map/ppermute | solution.py:488
  31.9 2.6 %collective-permute-start.5 = (bf16[80,256]{1,0:T(8,128)(2,1)S(1)}, bf16[80,256]{1,0:T(8,128)(2,1)S(1)}, u32[]{:S(2)}, u32[]{:S(2)}) collective-permute-start(bf16[80,256]{1,0:T(8,128)(2,1)S(1)} %get-tuple-element.36.refs_0_), channel_id=1, source_target_pairs={{0,16},{2,18},{4,20},{6,22},{8,24},{10,26},{12,28},{14,30},{16,0},... | collective-permute-start | bytes 122888 | tf_op jit(solution)/shard_map/ppermute | solution.py:488
  34.5 0.0 collective-permute-start.6
  34.5 0.0 copy-done.10
  34.5 1.5 %blockwise.1 = (f32[384,512]{1,0:T(8,128)S(1)}, bf16[384,256]{1,0:T(8,128)(2,1)S(1)}, f32[64,256]{1,0:T(8,128)S(1)}) custom-call(bf16[384,256]{1,0:T(8,128)(2,1)S(1)} %get-tuple-element.43.query, bf16[384,256]{1,0:T(8,128)(2,1)S(1)} %get-tuple-element.44.key, bf16[384,512]{1,0:T(8,128)(2,1)S(1)} %get-tuple-element.45.val, ...), custom_call_target="tpu_custom_call" | custom-call | flops 1207959552 | bytes 1048576 | tf_op jit(solution)/shard_map/blockwise/pallas_call | solution.py:29
  36.0 0.0 collective-permute-done.4.refs_1_
  36.0 1.4 %collective-permute-done.5.refs_2_ = bf16[80,256]{1,0:T(8,128)(2,1)S(1)} collective-permute-done((bf16[80,256]{1,0:T(8,128)(2,1)S(1)}, bf16[80,256]{1,0:T(8,128)(2,1)S(1)}, u32[]{:S(2)}, u32[]{:S(2)}) %collective-permute-start.5) | collective-permute-done | bytes 40992 | tf_op jit(solution)/shard_map/ppermute | solution.py:488
  37.4 2.9 %collective-permute-done.6.refs_3_ = bf16[80,256]{1,0:T(8,128)(2,1)S(1)} collective-permute-done((bf16[80,256]{1,0:T(8,128)(2,1)S(1)}, bf16[80,256]{1,0:T(8,128)(2,1)S(1)}, u32[]{:S(2)}, u32[]{:S(2)}) %collective-permute-start.6) | collective-permute-done | bytes 40992 | tf_op jit(solution)/shard_map/ppermute | solution.py:488
  40.3 3.5 %partner_rows.1 = (bf16[192,2048]{1,0:T(8,128)(2,1)S(1)}, bf16[2,256,128]{2,1,0:T(8,128)(2,1)S(1)}, f32[8,512]{1,0:T(8,128)S(1)}) custom-call(s32[3]{0:T(128)S(1)} %add_add_fusion.place, bf16[80,256]{1,0:T(8,128)(2,1)S(1)} %get-tuple-element.36.refs_0_, bf16[80,256]{1,0:T(8,128)(2,1)S(1)} %collective-permute-done.4.refs_1_, ...), custom_call_target="tpu_custom_call" | custom-call | flops 805306368 | bytes 1048576 | tf_op jit(solution)/shard_map/partner_rows/pallas_call | solution.py:29
  43.8 0.1 collective-permute-start.7
  43.9 3.5 %own_rows.1 = f32[192,2048]{1,0:T(8,128)S(1)} custom-call(s32[3]{0:T(128)S(1)} %add_add_fusion.place, bf16[2,256,128]{2,1,0:T(8,128)(2,1)S(1)} %get-tuple-element.54.state, f32[8,512]{1,0:T(8,128)S(1)} %get-tuple-element.55.halo, f32[384,512]{1,0:T(8,128)S(1)} %get-tuple-element.49.refs_8_.raw, bf16[384,256]{1,0:T(8,128)(2,1)S(1)} %get-tuple-element.50.refs_9_.through, ...), custom_call_target="tpu_custom_call" | custom-call | flops 805306368 | bytes 1048576 | tf_op jit(solution)/shard_map/own_rows/pallas_call | solution.py:29
  47.4 0.0 collective-permute-done.7
  47.4 1.1 %add_convert_fusion = bf16[192,2048]{1,0:T(8,128)(2,1)} fusion(f32[192,2048]{1,0:T(8,128)S(1)} %own_rows.1, bf16[192,2048]{1,0:T(8,128)(2,1)S(1)} %collective-permute-done.7), kind=kLoop, calls=%fused_computation | loop fusion | flops 1179648 | bytes 3145728 | tf_op jit(solution)/shard_map/convert_element_type | solution.py:534
  (6 shorter events, 0.0 us)
Async XLA Ops:
  0.0 12.1 %collective-permute-start = (bf16[384,1024]{1,0:T(8,128)(2,1)}, bf16[384,1024]{1,0:T(8,128)(2,1)S(1)}, u32[]{:S(2)}, u32[]{:S(2)}) collective-permute-start(bf16[384,1024]{1,0:T(8,128)(2,1)} %tok.1), channel_id=1, source_target_pairs={{0,1},{1,0},{2,3},{3,2},{4,5},{5,4},{6,7},{7,6},{8,9},{9,8},{10,11... | collective-permute-start | bytes 2359304 | tf_op jit(solution)/shard_map/ppermute | solution.py:410
  2.2 1.2 %copy-start = (bf16[2048,256]{1,0:T(8,128)(2,1)S(1)}, bf16[2048,256]{1,0:T(8,128)(2,1)}, u32[]{:S(2)}) copy-start(bf16[2048,256]{1,0:T(8,128)(2,1)} %refs_0_.3) | copy-start | bytes 3145732
  3.4 1.2 %copy-start.2 = (bf16[2048,256]{1,0:T(8,128)(2,1)S(1)}, bf16[2048,256]{1,0:T(8,128)(2,1)}, u32[]{:S(2)}) copy-start(bf16[2048,256]{1,0:T(8,128)(2,1)} %refs_1_.3) | copy-start | bytes 3145732
  4.7 1.1 %copy-start.4 = (bf16[384,1024]{1,0:T(8,128)(2,1)S(1)}, bf16[384,1024]{1,0:T(8,128)(2,1)}, u32[]{:S(2)}) copy-start(bf16[384,1024]{1,0:T(8,128)(2,1)} %tok.1) | copy-start | bytes 2359300
  5.8 0.7 %copy-start.5 = (f32[2048]{0:T(1024)S(1)}, f32[2048]{0:T(1024)}, u32[]{:S(2)}) copy-start(f32[2048]{0:T(1024)} %param.18) | copy-start | bytes 24580
  6.5 5.6 %copy-start.1 = (bf16[2048,256]{1,0:T(8,128)(2,1)S(1)}, bf16[2048,256]{1,0:T(8,128)(2,1)}, u32[]{:S(2)}) copy-start(bf16[2048,256]{1,0:T(8,128)(2,1)} %refs_0_.3) | copy-start | bytes 3145732
  6.5 5.6 %copy-start.3 = (bf16[2048,256]{1,0:T(8,128)(2,1)S(1)}, bf16[2048,256]{1,0:T(8,128)(2,1)}, u32[]{:S(2)}) copy-start(bf16[2048,256]{1,0:T(8,128)(2,1)} %refs_1_.3) | copy-start | bytes 3145732
  6.5 5.6 %copy-start.7 = (f32[256]{0:T(256)S(1)}, f32[256]{0:T(256)}, u32[]{:S(2)}) copy-start(f32[256]{0:T(256)} %param.28) | copy-start | bytes 3076
  12.1 11.0 %copy-start.6 = (bf16[3,512]{1,0:T(4,128)(2,1)S(1)}, bf16[3,512]{1,0:T(4,128)(2,1)}, u32[]{:S(2)}) copy-start(bf16[3,512]{1,0:T(4,128)(2,1)} %taps.3) | copy-start | bytes 9220
  12.1 11.0 %copy-start.9 = (bf16[2048,256]{1,0:T(8,128)(2,1)S(1)}, bf16[2048,256]{1,0:T(8,128)(2,1)}, u32[]{:S(2)}) copy-start(bf16[2048,256]{1,0:T(8,128)(2,1)} %wq.1) | copy-start | bytes 3145732
  19.0 10.1 %collective-permute-start.1 = (bf16[80,256]{1,0:T(8,128)(2,1)S(1)}, bf16[80,256]{1,0:T(8,128)(2,1)S(1)}, u32[]{:S(2)}, u32[]{:S(2)}) collective-permute-start(bf16[80,256]{1,0:T(8,128)(2,1)S(1)} %get-tuple-element.35.refs_0_), channel_id=1, source_target_pairs={{0,2},{2,0},{4,6},{6,4},{8,10},{10,8},{12,14},{14,12},{16,18},{18,... | collective-permute-start | bytes 122888 | tf_op jit(solution)/shard_map/ppermute | solution.py:488
  21.6 7.5 %collective-permute-start.2 = (bf16[80,256]{1,0:T(8,128)(2,1)S(1)}, bf16[80,256]{1,0:T(8,128)(2,1)S(1)}, u32[]{:S(2)}, u32[]{:S(2)}) collective-permute-start(bf16[80,256]{1,0:T(8,128)(2,1)S(1)} %get-tuple-element.35.refs_0_), channel_id=1, source_target_pairs={{0,4},{2,6},{4,0},{6,2},{8,12},{10,14},{12,8},{14,10},{16,20},{18,... | collective-permute-start | bytes 122888 | tf_op jit(solution)/shard_map/ppermute | solution.py:488
  23.1 6.0 %collective-permute-start.3 = (bf16[80,256]{1,0:T(8,128)(2,1)S(1)}, bf16[80,256]{1,0:T(8,128)(2,1)S(1)}, u32[]{:S(2)}, u32[]{:S(2)}) collective-permute-start(bf16[80,256]{1,0:T(8,128)(2,1)S(1)} %get-tuple-element.35.refs_0_), channel_id=1, source_target_pairs={{0,6},{2,4},{4,2},{6,0},{8,14},{10,12},{12,10},{14,8},{16,22},{18,... | collective-permute-start | bytes 122888 | tf_op jit(solution)/shard_map/ppermute | solution.py:488
  23.1 1.4 %copy-start.8 = (bf16[384,2048]{1,0:T(8,128)(2,1)S(1)}, bf16[384,2048]{1,0:T(8,128)(2,1)}, u32[]{:S(2)}) copy-start(bf16[384,2048]{1,0:T(8,128)(2,1)} %get-tuple-element.40.full) | copy-start | bytes 4718596
  24.5 10.0 %copy-start.10 = (f32[8,32,64]{2,1,0:T(8,128)S(1)}, f32[8,32,64]{2,1,0:T(8,128)}, u32[]{:S(2)}) copy-start(f32[8,32,64]{2,1,0:T(8,128)} %param.30) | copy-start | bytes 196612
  29.8 6.2 %collective-permute-start.4 = (bf16[80,256]{1,0:T(8,128)(2,1)S(1)}, bf16[80,256]{1,0:T(8,128)(2,1)S(1)}, u32[]{:S(2)}, u32[]{:S(2)}) collective-permute-start(bf16[80,256]{1,0:T(8,128)(2,1)S(1)} %get-tuple-element.36.refs_0_), channel_id=1, source_target_pairs={{0,8},{2,10},{4,12},{6,14},{8,0},{10,2},{12,4},{14,6},{16,24},{18,... | collective-permute-start | bytes 122888 | tf_op jit(solution)/shard_map/ppermute | solution.py:488
  31.9 5.5 %collective-permute-start.5 = (bf16[80,256]{1,0:T(8,128)(2,1)S(1)}, bf16[80,256]{1,0:T(8,128)(2,1)S(1)}, u32[]{:S(2)}, u32[]{:S(2)}) collective-permute-start(bf16[80,256]{1,0:T(8,128)(2,1)S(1)} %get-tuple-element.36.refs_0_), channel_id=1, source_target_pairs={{0,16},{2,18},{4,20},{6,22},{8,24},{10,26},{12,28},{14,30},{16,0},... | collective-permute-start | bytes 122888 | tf_op jit(solution)/shard_map/ppermute | solution.py:488
  34.5 5.8 %collective-permute-start.6 = (bf16[80,256]{1,0:T(8,128)(2,1)S(1)}, bf16[80,256]{1,0:T(8,128)(2,1)S(1)}, u32[]{:S(2)}, u32[]{:S(2)}) collective-permute-start(bf16[80,256]{1,0:T(8,128)(2,1)S(1)} %get-tuple-element.36.refs_0_), channel_id=1, source_target_pairs={{0,24},{2,26},{4,28},{6,30},{8,16},{10,18},{12,20},{14,22},{16,8},... | collective-permute-start | bytes 122888 | tf_op jit(solution)/shard_map/ppermute | solution.py:488
  43.8 3.6 %collective-permute-start.7 = (bf16[192,2048]{1,0:T(8,128)(2,1)S(1)}, bf16[192,2048]{1,0:T(8,128)(2,1)S(1)}, u32[]{:S(2)}, u32[]{:S(2)}) collective-permute-start(bf16[192,2048]{1,0:T(8,128)(2,1)S(1)} %get-tuple-element.56), channel_id=1, source_target_pairs={{0,1},{1,0},{2,3},{3,2},{4,5},{5,4},{6,7},{7,6},{8,9},{9,8},{10,11... | collective-permute-start | bytes 2359304 | tf_op jit(solution)/shard_map/ppermute | solution.py:526

commit v2 on v1

--- a/solution.py
+++ b/solution.py
@@ -16,7 +16,7 @@
 TN = (((0,), (0,)), ((), ()))
 VMEM = pl.BlockSpec(memory_space=pltpu.VMEM)
 SMEM = pl.BlockSpec(memory_space=pltpu.SMEM)
-HBM = pl.BlockSpec(memory_space=pl.ANY)
+HBM = pl.BlockSpec(memory_space=pltpu.HBM)
 EXTRA_ROWS = 16
 
 
@@ -24,7 +24,7 @@
     return jnp.dot(a, b, preferred_element_type=F32)
 
 
-def call(body, outs, ins, flops, scratch=(), limit=48 << 20, name=None):
+def call(body, outs, ins, flops, scratch=(), limit=12 << 20, name=None):
     specs = [s for _, s in ins]
     return pl.pallas_call(
         body,
@@ -35,7 +35,7 @@
         compiler_params=pltpu.CompilerParams(vmem_limit_bytes=limit),
         cost_estimate=pl.CostEstimate(flops=flops, bytes_accessed=1 << 20, transcendentals=0),
         name=name,
-    )(*[a for a, _ in ins])
+    )(*[pltpu.with_memory_space_constraint(a, pltpu.HBM) if s is HBM else a for a, s in ins])
 
 
 def weight_copies(hbm, buf, sems, row, rows):
@@ -61,23 +61,33 @@
     return r == c
 
 
-def own_half(tp, tok, gain, extra, *refs):
-    weights, (acc, xg, ssq, wide), (buf, sems) = refs[:5], refs[5:9], refs[9:]
+def own_half(tp, tok_hbm, gain_hbm, extra_hbm, *refs):
+    weights, (acc, xg, ssq, wide, rest) = refs[:5], refs[5:10]
+    buf, sems, tok, gain, extra, small = refs[10:]
     half = tok.shape[1]
     at = pl.multiple_of(tp[0] * half, half)
-    copies = weight_copies(weights, buf, sems, at, half)
-    for c in copies:
+    loads = [
+        pltpu.make_async_copy(src, dst, small.at[i])
+        for i, (src, dst) in enumerate([(tok_hbm, tok), (gain_hbm, gain), (extra_hbm, extra)])
+    ]
+    copies = weight_copies(weights, buf, sems.at[0], at, half)
+    away = pl.multiple_of((1 - tp[0]) * half, half)
+    ahead = weight_copies(weights, rest, sems.at[1], away, half)
+    for c in loads + copies + ahead:
         c.start()
+    for c in loads:
+        c.wait()
     x = tok[...].astype(F32)
     ssq[...] = jnp.broadcast_to(jnp.sum(x * x, axis=1, keepdims=True), ssq.shape)
     xg[...] = (x * gain[:, pl.ds(at, half)]).astype(BF16)
-    heads = extra.shape[1]
+    heads = extra.shape[0]
     lanes = wide.shape[1]
     r = lax.broadcasted_iota(jnp.int32, (heads, lanes), 0)
     c = lax.broadcasted_iota(jnp.int32, (heads, lanes), 1) // (lanes // heads)
-    wide[...] = jnp.dot(
+    wide[...] = lax.dot_general(
         extra[...],
         (r == c).astype(F32),
+        TN,
         precision=lax.Precision.HIGHEST,
         preferred_element_type=F32,
     )
@@ -88,17 +98,16 @@
         c.wait()
         acc[:, at : at + cols] = dot(left, buf[:, at : at + cols])
         at += cols
-
-
-def other_half(tp, tok, gain, bias, acc, xg, ssq, wide, *refs):
-    weights = refs[:5]
-    full, scale, key, val, cum, base, prod, own, send = refs[5:14]
-    buf, sems = refs[14:]
+    for c in ahead:
+        c.wait()
+
+
+def other_half(
+    tp, tok, gain, bias, acc, xg, ssq, wide, wnext,
+    full, scale, key, val, cum, base, prod, own, send,
+):
     rows, half = tok.shape
     at = pl.multiple_of((1 - tp[0]) * half, half)
-    copies = weight_copies(weights, buf, sems, at, half)
-    for c in copies:
-        c.start()
     x = tok[...].astype(F32)
     power = (ssq[:, :1] + jnp.sum(x * x, axis=1, keepdims=True)) * (0.5 / half)
     r = jnp.broadcast_to(lax.rsqrt(power + NORM_EPS), scale.shape)
@@ -107,17 +116,14 @@
     full[:, pl.ds(at, half)] = left
     full[:, pl.ds(pl.multiple_of(tp[0] * half, half), half)] = xg[...]
 
-    def project(i, lo, hi):
-        copies[i].wait()
-        s = acc[:, lo:hi] + dot(left, buf[:, lo:hi])
+    def project(lo, hi):
+        s = acc[:, lo:hi] + dot(left, wnext[:, lo:hi])
         return (s * tile_lanes(r, hi - lo)).astype(BF16)
 
-    kw = weights[0].shape[1]
-    vw = weights[2].shape[1]
-    cw = weights[3].shape[1]
-    k = project(0, 0, kw)
+    kw, vw, cw = key.shape[1], val.shape[1], prod.shape[1]
+    k = project(0, kw)
     key[...] = k
-    f = project(1, kw, 2 * kw).astype(F32) + bias[...]
+    f = project(kw, 2 * kw).astype(F32) + bias[...]
     log = (jnp.minimum(f, 0.0) - jnp.log1p(jnp.exp(-jnp.abs(f)))) * (1.0 / GATE_SOFTNESS)
     log = log + wide[...]
     hi = log.astype(BF16)
@@ -144,7 +150,7 @@
         s = slice(b * BLOCK, (b + 1) * BLOCK)
         decayed.append((kf[s] * jnp.exp((running - starts[b]) - cum[s, :])).astype(BF16))
     decayed = jnp.concatenate(decayed, axis=0)
-    val[...] = project(2, 2 * kw, 2 * kw + vw)
+    val[...] = project(2 * kw, 2 * kw + vw)
     dv = own.shape[0]
     group = vw // 256
     for g in range(group):
@@ -155,9 +161,9 @@
             preferred_element_type=F32,
         )
         own[:, g * 128 : (g + 1) * 128] = fold(m, dv)
-    at = 2 * kw + vw
-    c_in = project(3, at, at + cw).astype(F32)
-    h_in = project(4, at + cw, at + 2 * cw).astype(F32)
+    lo = 2 * kw + vw
+    c_in = project(lo, lo + cw).astype(F32)
+    h_in = project(lo + cw, lo + 2 * cw).astype(F32)
     p = c_in * h_in
     p = p.astype(BF16)
     prod[...] = p
@@ -244,7 +250,7 @@
     conv[...] = (b.astype(F32) * total).astype(BF16)
     query[...] = project(wq)
     g = project(wg).astype(F32)
-    gate[...] = g * jax.nn.sigmoid(g) * gain[...]
+    gate[...] = g * jax.nn.sigmoid(g) * tile_lanes(gain[...], g.shape[1])
 
 
 def blockwise(key_dim, query, key, val, cum, base, start, raw, through, first):
@@ -418,13 +424,26 @@
         convolution_input_weight,
     )
     width = sum(w.shape[1] for w in early)
-    buffers = [pltpu.VMEM((half, width), BF16), pltpu.SemaphoreType.DMA((5,))]
+    extra = extra_logarithm_decay.T
+    buffers = [
+        pltpu.VMEM((half, width), BF16),
+        pltpu.SemaphoreType.DMA((2, 5)),
+        pltpu.VMEM(tokens.shape, BF16),
+        pltpu.VMEM(gain.shape, F32),
+        pltpu.VMEM(extra.shape, F32),
+        pltpu.SemaphoreType.DMA((3,)),
+    ]
     flops = 2 * rows * half * width
-    acc, xg, ssq, wide = call(
+    acc, xg, ssq, wide, rest = call(
         own_half,
-        [((rows, width), F32), ((rows, half), BF16), ((rows, 128), F32), ((rows, kw), F32)],
-        [(tp1, SMEM), (tokens, VMEM), (gain, VMEM), (extra_logarithm_decay, VMEM)]
-        + [(w, HBM) for w in early],
+        [
+            ((rows, width), F32),
+            ((rows, half), BF16),
+            ((rows, 128), F32),
+            ((rows, kw), F32),
+            ((half, width), BF16),
+        ],
+        [(tp1, SMEM), (tokens, HBM), (gain, HBM), (extra, HBM)] + [(w, HBM) for w in early],
         flops,
         buffers,
         name="own_half",
@@ -443,10 +462,8 @@
             ((dv + EXTRA_ROWS, kw), BF16),
         ],
         [(tp1, SMEM), (other, VMEM), (gain, VMEM), (forget_gate_bias.reshape(1, -1), VMEM)]
-        + [(a, VMEM) for a in (acc, xg, ssq, wide)]
-        + [(w, HBM) for w in early],
+        + [(a, VMEM) for a in (acc, xg, ssq, wide, rest)],
         flops,
-        buffers,
         name="other_half",
     )
     query, outer, gate, conv = call(
@@ -457,7 +474,7 @@
             (scale, VMEM),
             (prod, VMEM),
             (convolution_kernel_taps, VMEM),
-            (jnp.tile(head_norm_gain.reshape(1, -1), (1, heads)), VMEM),
+            (head_norm_gain.reshape(1, -1), VMEM),
             (query_weight_matrix, VMEM),
             (outer_gate_weight, VMEM),
             (attention_gate_weight, VMEM),

time: 48.9 us -> 35.7 us (0.73)
  Pallas kernels: 26.2 us -> 18 us
  local copies, waits for them, and re-layouts: 7.3 us -> 0.06 us
  waiting for transfers between devices: 4.27 us -> 7.03 us
    pallas_call x7, Pallas kernels: 26.2 us -> 18 us  [call(): pl.pallas_call(body, out_shape=[jax.ShapeDtypeStruct(s, d) for s, d in ou...]
    unnamed x23 -> x20, local copies, waits for them, and re-layouts: 6.54 us -> 0.05 us
    ppermute x6, waiting for transfers between devices: 4.26 us -> 6.55 us  [on_device(): lax.ppermute(send, 'sp', [(i, i ^ j * stride) for i in range(n_sp)])]
    another operation x2 -> x0, local copies, waits for them, and re-layouts: 0.74 us -> none  [on_device(): jnp.tile(head_norm_gain.reshape(1, -1), (1, heads))]
  transfers between devices with their start and end apart: 8 -> 8, of which waited for: 2 -> 5; matrix products, arithmetic and copies ran while one was open for 4% -> 0% of each run, Pallas kernels for 31% -> 36%
where the time goes in v2:
time: 35.7 us; the launch traced here: 35.6 us
  Pallas kernels  18 us (50%)
  starting transfers between devices  9.1 us (25%)
  waiting for transfers between devices  7.03 us (20%)
  other arithmetic  1.21 us (3%)
    pallas_call x7, Pallas kernels, call(): pl.pallas_call(body, out_shape=[jax.ShapeDtypeStruct(s, d) for s, d in ou...  18 us
    ppermute x6, starting transfers between devices, on_device(): lax.ppermute(send, 'sp', [(i, i ^ j * stride) for i in range(n_sp)])  8.54 us
    ppermute x6, waiting for transfers between devices, on_device(): lax.ppermute(send, 'sp', [(i, i ^ j * stride) for i in range(n_sp)])  6.55 us
    convert_element_type x1, other arithmetic, on_device(): return (mine + got.astype(F32)).astype(BF16)  1.06 us
  transfers between devices with their start and end apart: 8, of which 5 were waited for; matrix products, arithmetic and copies ran while one was open for 0% of the time, Pallas kernels for 36%

profile of v2, /device:TPU:0, one launch (start us, length us, event | category | flops | bytes accessed | tf_op | source)
XLA Modules:
  0.0 35.6 jit_solution(3732175776963026335)
XLA Ops:
  0.0 0.5 %collective-permute-start = (bf16[384,1024]{1,0:T(8,128)(2,1)}, bf16[384,1024]{1,0:T(8,128)(2,1)S(1)}, u32[]{:S(2)}, u32[]{:S(2)}) collective-permute-start(bf16[384,1024]{1,0:T(8,128)(2,1)} %tok_hbm.1), channel_id=1, source_target_pairs={{0,1},{1,0},{2,3},{3,2},{4,5},{5,4},{6,7},{7,6},{8,9},{9,8},{10,11... | collective-permute-start | bytes 2359304 | tf_op jit(solution)/shard_map/ppermute | solution.py:416
  0.5 0.1 add_add_fusion.1.place
  0.6 0.1 add_add_fusion.place
  0.6 0.0 copy-start.2
  0.6 0.0 copy-start.4
  0.6 7.1 %own_half.1 = (f32[384,2048]{1,0:T(8,128)S(1)}, bf16[384,1024]{1,0:T(8,128)(2,1)S(1)}, f32[384,128]{1,0:T(8,128)S(1)}, f32[384,256]{1,0:T(8,128)S(1)}, bf16[1024,2048]{1,0:T(8,128)(2,1)S(1)}) custom-call(s32[1]{0:T(128)} %bitcast.2.tp, bf16[384,1024]{1,0:T(8,128)(2,1)} %tok_hbm.1, f32[1,2048]{1,0:T(1,128)} %bitcast.9, f32[8,384]{1,0:T(8,128)} %bitcast.14, ...), custom_call_target="tpu_custom_call" | custom-call | flops 1610612736 | bytes 1048576 | tf_op jit(solution)/shard_map/own_half/pallas_call | solution.py:29
  7.7 0.0 collective-permute-done.tok
  7.7 0.0 copy-done.2
  7.8 0.0 copy-done.4
  7.8 0.0 copy-start.3
  7.8 0.0 copy-start.5
  7.8 0.0 copy-start.6
  7.8 0.0 copy-start.7
  7.8 0.0 copy-start.9
  7.8 2.8 %other_half.1 = (bf16[384,2048]{1,0:T(8,128)(2,1)S(1)}, f32[384,128]{1,0:T(8,128)S(1)}, bf16[384,256]{1,0:T(8,128)(2,1)S(1)}, bf16[384,512]{1,0:T(8,128)(2,1)S(1...) custom-call(s32[1]{0:T(128)} %bitcast.2.tp, ...), custom_call_target="tpu_custom_call" | custom-call | flops 1610612736 | bytes 1048576 | tf_op jit(solution)/shard_map/other_half/pallas_call | solution.py:29
  10.7 2.5 %collective-permute-start.1 = (bf16[80,256]{1,0:T(8,128)(2,1)S(1)}, bf16[80,256]{1,0:T(8,128)(2,1)S(1)}, u32[]{:S(2)}, u32[]{:S(2)}) collective-permute-start(bf16[80,256]{1,0:T(8,128)(2,1)S(1)} %get-tuple-element.37.refs_0_), channel_id=1, source_target_pairs={{0,2},{2,0},{4,6},{6,4},{8,10},{10,8},{12,14},{14,12},{16,18},{18,... | collective-permute-start | bytes 122888 | tf_op jit(solution)/shard_map/ppermute | solution.py:505
  13.2 1.5 %collective-permute-start.2 = (bf16[80,256]{1,0:T(8,128)(2,1)S(1)}, bf16[80,256]{1,0:T(8,128)(2,1)S(1)}, u32[]{:S(2)}, u32[]{:S(2)}) collective-permute-start(bf16[80,256]{1,0:T(8,128)(2,1)S(1)} %get-tuple-element.37.refs_0_), channel_id=1, source_target_pairs={{0,4},{2,6},{4,0},{6,2},{8,12},{10,14},{12,8},{14,10},{16,20},{18,... | collective-permute-start | bytes 122888 | tf_op jit(solution)/shard_map/ppermute | solution.py:505
  14.7 0.0 collective-permute-start.3
  14.7 0.0 copy-done.3
  14.7 0.0 copy-done.5
  14.8 0.0 copy-done.6
  14.8 0.0 copy-done.7
  14.8 0.0 copy-done.9
  14.8 0.0 copy-start.8
  14.8 2.3 %late_half.1 = (bf16[384,256]{1,0:T(8,128)(2,1)S(1)}, bf16[384,512]{1,0:T(8,128)(2,1)S(1)}, f32[384,512]{1,0:T(8,128)S(1)}, bf16[384,512]{1,0:T(8,128)(2,1)S(1)}) custom-call(bf16[384,2048]{1,0:T(8,128)(2,1)S(1)} %get-tuple-element.42.full, f32[384,128]{1,0:T(8,128)S(1)} %get-tuple-element.43.scale, bf16[384,512]{1,0:T(8,128)(2,1)S(1)} %get-tuple-element.44.prod.refs_13_, ...), custom_call_target="tpu_custom_call" | custom-call | flops 2013265920 | bytes 1048576 | tf_op jit(solution)/shard_map/late_half/pallas_call | solution.py:29
  17.1 0.0 collective-permute-done.1.refs_1_
  17.1 0.1 collective-permute-done.2.refs_2_
  17.2 2.4 %collective-permute-done.3.refs_3_ = bf16[80,256]{1,0:T(8,128)(2,1)S(1)} collective-permute-done((bf16[80,256]{1,0:T(8,128)(2,1)S(1)}, bf16[80,256]{1,0:T(8,128)(2,1)S(1)}, u32[]{:S(2)}, u32[]{:S(2)}) %collective-permute-start.3) | collective-permute-done | bytes 40992 | tf_op jit(solution)/shard_map/ppermute | solution.py:505
  19.6 0.6 %join_round.1 = (bf16[80,256]{1,0:T(8,128)(2,1)S(1)}, f32[64,256]{1,0:T(8,128)S(1)}, f32[8,256]{1,0:T(8,128)S(1)}, f32[16,256]{1,0:T(8,128)S(1)}) custom-call(s32[3]{0:T(128)S(1)} %add_add_fusion.1.place, bf16[80,256]{1,0:T(8,128)(2,1)S(1)} %get-tuple-element.37.refs_0_, bf16[80,256]{1,0:T(8,128)(2,1)S(1)} %collective-permute-done.1.refs_1_, ...), custom_call_target="tpu_custom_call" | custom-call | flops 1048576 | bytes 1048576 | tf_op jit(solution)/shard_map/join_round/pallas_call | solution.py:29
  20.3 1.6 %collective-permute-start.4 = (bf16[80,256]{1,0:T(8,128)(2,1)S(1)}, bf16[80,256]{1,0:T(8,128)(2,1)S(1)}, u32[]{:S(2)}, u32[]{:S(2)}) collective-permute-start(bf16[80,256]{1,0:T(8,128)(2,1)S(1)} %get-tuple-element.38.refs_0_), channel_id=1, source_target_pairs={{0,8},{2,10},{4,12},{6,14},{8,0},{10,2},{12,4},{14,6},{16,24},{18,... | collective-permute-start | bytes 122888 | tf_op jit(solution)/shard_map/ppermute | solution.py:505
  21.9 2.6 %collective-permute-start.5 = (bf16[80,256]{1,0:T(8,128)(2,1)S(1)}, bf16[80,256]{1,0:T(8,128)(2,1)S(1)}, u32[]{:S(2)}, u32[]{:S(2)}) collective-permute-start(bf16[80,256]{1,0:T(8,128)(2,1)S(1)} %get-tuple-element.38.refs_0_), channel_id=1, source_target_pairs={{0,16},{2,18},{4,20},{6,22},{8,24},{10,26},{12,28},{14,30},{16,0},... | collective-permute-start | bytes 122888 | tf_op jit(solution)/shard_map/ppermute | solution.py:505
  24.5 0.2 collective-permute-start.6
  24.7 0.0 copy-done.8
  24.7 0.0 copy-start
  24.7 0.0 copy-start.1
  24.7 1.5 %blockwise.1 = (f32[384,512]{1,0:T(8,128)S(1)}, bf16[384,256]{1,0:T(8,128)(2,1)S(1)}, f32[64,256]{1,0:T(8,128)S(1)}) custom-call(bf16[384,256]{1,0:T(8,128)(2,1)S(1)} %get-tuple-element.45.query, bf16[384,256]{1,0:T(8,128)(2,1)S(1)} %get-tuple-element.46.key, bf16[384,512]{1,0:T(8,128)(2,1)S(1)} %get-tuple-element.47.val, ...), custom_call_target="tpu_custom_call" | custom-call | flops 1207959552 | bytes 1048576 | tf_op jit(solution)/shard_map/blockwise/pallas_call | solution.py:29
  26.3 0.0 collective-permute-done.4.refs_1_
  26.3 1.4 %collective-permute-done.5.refs_2_ = bf16[80,256]{1,0:T(8,128)(2,1)S(1)} collective-permute-done((bf16[80,256]{1,0:T(8,128)(2,1)S(1)}, bf16[80,256]{1,0:T(8,128)(2,1)S(1)}, u32[]{:S(2)}, u32[]{:S(2)}) %collective-permute-start.5) | collective-permute-done | bytes 40992 | tf_op jit(solution)/shard_map/ppermute | solution.py:505
  27.7 2.6 %collective-permute-done.6.refs_3_ = bf16[80,256]{1,0:T(8,128)(2,1)S(1)} collective-permute-done((bf16[80,256]{1,0:T(8,128)(2,1)S(1)}, bf16[80,256]{1,0:T(8,128)(2,1)S(1)}, u32[]{:S(2)}, u32[]{:S(2)}) %collective-permute-start.6) | collective-permute-done | bytes 40992 | tf_op jit(solution)/shard_map/ppermute | solution.py:505
  30.3 0.0 copy-done
  30.3 0.0 copy-done.1
  30.3 1.8 %partner_rows.1 = (bf16[192,2048]{1,0:T(8,128)(2,1)S(1)}, bf16[2,256,128]{2,1,0:T(8,128)(2,1)S(1)}, f32[8,512]{1,0:T(8,128)S(1)}) custom-call(s32[3]{0:T(128)S(1)} %add_add_fusion.place, bf16[80,256]{1,0:T(8,128)(2,1)S(1)} %get-tuple-element.38.refs_0_, bf16[80,256]{1,0:T(8,128)(2,1)S(1)} %collective-permute-done.4.refs_1_, ...), custom_call_target="tpu_custom_call" | custom-call | flops 805306368 | bytes 1048576 | tf_op jit(solution)/shard_map/partner_rows/pallas_call | solution.py:29
  32.2 0.1 collective-permute-start.7
  32.3 1.8 %own_rows.1 = f32[192,2048]{1,0:T(8,128)S(1)} custom-call(s32[3]{0:T(128)S(1)} %add_add_fusion.place, bf16[2,256,128]{2,1,0:T(8,128)(2,1)S(1)} %get-tuple-element.56.state, f32[8,512]{1,0:T(8,128)S(1)} %get-tuple-element.57.halo, f32[384,512]{1,0:T(8,128)S(1)} %get-tuple-element.51.refs_8_.raw, bf16[384,256]{1,0:T(8,128)(2,1)S(1)} %get-tuple-element.52.refs_9_.through, ...), custom_call_target="tpu_custom_call" | custom-call | flops 805306368 | bytes 1048576 | tf_op jit(solution)/shard_map/own_rows/pallas_call | solution.py:29
  34.0 0.5 %collective-permute-done.7 = bf16[192,2048]{1,0:T(8,128)(2,1)S(1)} collective-permute-done((bf16[192,2048]{1,0:T(8,128)(2,1)S(1)}, bf16[192,2048]{1,0:T(8,128)(2,1)S(1)}, u32[]{:S(2)}, u32[]{:S(2)}) %collective-permute-start.7) | collective-permute-done | bytes 786464 | tf_op jit(solution)/shard_map/ppermute | solution.py:543
  34.5 1.1 %add_convert_fusion = bf16[192,2048]{1,0:T(8,128)(2,1)} fusion(f32[192,2048]{1,0:T(8,128)S(1)} %own_rows.1, bf16[192,2048]{1,0:T(8,128)(2,1)S(1)} %collective-permute-done.7), kind=kLoop, calls=%fused_computation | loop fusion | flops 1179648 | bytes 3145728 | tf_op jit(solution)/shard_map/convert_element_type | solution.py:551
  (3 shorter events, 0.0 us)
Async XLA Ops:
  0.0 7.7 %collective-permute-start = (bf16[384,1024]{1,0:T(8,128)(2,1)}, bf16[384,1024]{1,0:T(8,128)(2,1)S(1)}, u32[]{:S(2)}, u32[]{:S(2)}) collective-permute-start(bf16[384,1024]{1,0:T(8,128)(2,1)} %tok_hbm.1), channel_id=1, source_target_pairs={{0,1},{1,0},{2,3},{3,2},{4,5},{5,4},{6,7},{7,6},{8,9},{9,8},{10,11... | collective-permute-start | bytes 2359304 | tf_op jit(solution)/shard_map/ppermute | solution.py:416
  0.6 7.1 %copy-start.2 = (f32[2048]{0:T(1024)S(1)}, f32[2048]{0:T(1024)}, u32[]{:S(2)}) copy-start(f32[2048]{0:T(1024)} %param.18) | copy-start | bytes 24580
  0.6 7.1 %copy-start.4 = (f32[256]{0:T(256)S(1)}, f32[256]{0:T(256)}, u32[]{:S(2)}) copy-start(f32[256]{0:T(256)} %param.28) | copy-start | bytes 3076
  7.8 7.0 %copy-start.3 = (bf16[3,512]{1,0:T(4,128)(2,1)S(1)}, bf16[3,512]{1,0:T(4,128)(2,1)}, u32[]{:S(2)}) copy-start(bf16[3,512]{1,0:T(4,128)(2,1)} %taps.3) | copy-start | bytes 9220
  7.8 7.0 %copy-start.5 = (bf16[2048,512]{1,0:T(8,128)(2,1)S(1)}, bf16[2048,512]{1,0:T(8,128)(2,1)}, u32[]{:S(2)}) copy-start(bf16[2048,512]{1,0:T(8,128)(2,1)} %wb.1) | copy-start | bytes 6291460
  7.8 7.0 %copy-start.6 = (bf16[2048,512]{1,0:T(8,128)(2,1)S(1)}, bf16[2048,512]{1,0:T(8,128)(2,1)}, u32[]{:S(2)}) copy-start(bf16[2048,512]{1,0:T(8,128)(2,1)} %wg.1) | copy-start | bytes 6291460
  7.8 7.0 %copy-start.7 = (bf16[2048,256]{1,0:T(8,128)(2,1)S(1)}, bf16[2048,256]{1,0:T(8,128)(2,1)}, u32[]{:S(2)}) copy-start(bf16[2048,256]{1,0:T(8,128)(2,1)} %wq.1) | copy-start | bytes 3145732
  7.8 6.9 %copy-start.9 = (f32[64]{0:T(128)S(1)}, f32[64]{0:T(128)}, u32[]{:S(2)}) copy-start(f32[64]{0:T(128)} %param.31) | copy-start | bytes 772
  10.7 6.4 %collective-permute-start.1 = (bf16[80,256]{1,0:T(8,128)(2,1)S(1)}, bf16[80,256]{1,0:T(8,128)(2,1)S(1)}, u32[]{:S(2)}, u32[]{:S(2)}) collective-permute-start(bf16[80,256]{1,0:T(8,128)(2,1)S(1)} %get-tuple-element.37.refs_0_), channel_id=1, source_target_pairs={{0,2},{2,0},{4,6},{6,4},{8,10},{10,8},{12,14},{14,12},{16,18},{18,... | collective-permute-start | bytes 122888 | tf_op jit(solution)/shard_map/ppermute | solution.py:505
  13.2 4.0 %collective-permute-start.2 = (bf16[80,256]{1,0:T(8,128)(2,1)S(1)}, bf16[80,256]{1,0:T(8,128)(2,1)S(1)}, u32[]{:S(2)}, u32[]{:S(2)}) collective-permute-start(bf16[80,256]{1,0:T(8,128)(2,1)S(1)} %get-tuple-element.37.refs_0_), channel_id=1, source_target_pairs={{0,4},{2,6},{4,0},{6,2},{8,12},{10,14},{12,8},{14,10},{16,20},{18,... | collective-permute-start | bytes 122888 | tf_op jit(solution)/shard_map/ppermute | solution.py:505
  14.7 4.9 %collective-permute-start.3 = (bf16[80,256]{1,0:T(8,128)(2,1)S(1)}, bf16[80,256]{1,0:T(8,128)(2,1)S(1)}, u32[]{:S(2)}, u32[]{:S(2)}) collective-permute-start(bf16[80,256]{1,0:T(8,128)(2,1)S(1)} %get-tuple-element.37.refs_0_), channel_id=1, source_target_pairs={{0,6},{2,4},{4,2},{6,0},{8,14},{10,12},{12,10},{14,8},{16,22},{18,... | collective-permute-start | bytes 122888 | tf_op jit(solution)/shard_map/ppermute | solution.py:505
  14.8 10.0 %copy-start.8 = (f32[8,32,64]{2,1,0:T(8,128)S(1)}, f32[8,32,64]{2,1,0:T(8,128)}, u32[]{:S(2)}) copy-start(f32[8,32,64]{2,1,0:T(8,128)} %param.30) | copy-start | bytes 196612
  20.3 6.0 %collective-permute-start.4 = (bf16[80,256]{1,0:T(8,128)(2,1)S(1)}, bf16[80,256]{1,0:T(8,128)(2,1)S(1)}, u32[]{:S(2)}, u32[]{:S(2)}) collective-permute-start(bf16[80,256]{1,0:T(8,128)(2,1)S(1)} %get-tuple-element.38.refs_0_), channel_id=1, source_target_pairs={{0,8},{2,10},{4,12},{6,14},{8,0},{10,2},{12,4},{14,6},{16,24},{18,... | collective-permute-start | bytes 122888 | tf_op jit(solution)/shard_map/ppermute | solution.py:505
  21.9 5.8 %collective-permute-start.5 = (bf16[80,256]{1,0:T(8,128)(2,1)S(1)}, bf16[80,256]{1,0:T(8,128)(2,1)S(1)}, u32[]{:S(2)}, u32[]{:S(2)}) collective-permute-start(bf16[80,256]{1,0:T(8,128)(2,1)S(1)} %get-tuple-element.38.refs_0_), channel_id=1, source_target_pairs={{0,16},{2,18},{4,20},{6,22},{8,24},{10,26},{12,28},{14,30},{16,0},... | collective-permute-start | bytes 122888 | tf_op jit(solution)/shard_map/ppermute | solution.py:505
  24.5 5.8 %collective-permute-start.6 = (bf16[80,256]{1,0:T(8,128)(2,1)S(1)}, bf16[80,256]{1,0:T(8,128)(2,1)S(1)}, u32[]{:S(2)}, u32[]{:S(2)}) collective-permute-start(bf16[80,256]{1,0:T(8,128)(2,1)S(1)} %get-tuple-element.38.refs_0_), channel_id=1, source_target_pairs={{0,24},{2,26},{4,28},{6,30},{8,16},{10,18},{12,20},{14,22},{16,8},... | collective-permute-start | bytes 122888 | tf_op jit(solution)/shard_map/ppermute | solution.py:505
  24.7 5.6 %copy-start = (bf16[512,2048]{1,0:T(8,128)(2,1)S(1)}, bf16[512,2048]{1,0:T(8,128)(2,1)}, u32[]{:S(2)}) copy-start(bf16[512,2048]{1,0:T(8,128)(2,1)} %wc.1) | copy-start | bytes 6291460
  24.7 5.6 %copy-start.1 = (bf16[512,2048]{1,0:T(8,128)(2,1)S(1)}, bf16[512,2048]{1,0:T(8,128)(2,1)}, u32[]{:S(2)}) copy-start(bf16[512,2048]{1,0:T(8,128)(2,1)} %wa.1) | copy-start | bytes 6291460
  32.2 2.4 %collective-permute-start.7 = (bf16[192,2048]{1,0:T(8,128)(2,1)S(1)}, bf16[192,2048]{1,0:T(8,128)(2,1)S(1)}, u32[]{:S(2)}, u32[]{:S(2)}) collective-permute-start(bf16[192,2048]{1,0:T(8,128)(2,1)S(1)} %get-tuple-element.58), channel_id=1, source_target_pairs={{0,1},{1,0},{2,3},{3,2},{4,5},{5,4},{6,7},{7,6},{8,9},{9,8},{10,11... | collective-permute-start | bytes 2359304 | tf_op jit(solution)/shard_map/ppermute | solution.py:543

commit v3 on v2

v3 whole, which is shorter than its diff:
```python
import functools

import jax
import jax.numpy as jnp
from jax import lax
from jax.experimental import pallas as pl
from jax.experimental.pallas import tpu as pltpu
from jax.sharding import PartitionSpec as P


BLOCK = 64
NORM_EPS = 1e-06
GATE_SOFTNESS = 16.0
F32 = jnp.float32
BF16 = jnp.bfloat16
NT = (((1,), (1,)), ((), ()))
TN = (((0,), (0,)), ((), ()))
VMEM = pl.BlockSpec(memory_space=pltpu.VMEM)
HBM = pl.BlockSpec(memory_space=pltpu.HBM)
EXTRA_ROWS = 16


def dot(a, b):
    return jnp.dot(a, b, preferred_element_type=F32)


def call(body, outs, ins, flops, scratch=(), limit=12 << 20):
    specs = [s for _, s in ins]
    return pl.pallas_call(
        body,
        out_shape=[jax.ShapeDtypeStruct(s, d) for s, d in outs],
        in_specs=specs,
        out_specs=[VMEM] * len(outs),
        scratch_shapes=list(scratch),
        compiler_params=pltpu.CompilerParams(vmem_limit_bytes=limit),
        cost_estimate=pl.CostEstimate(flops=flops, bytes_accessed=1 << 20, transcendentals=0),
    )(*[pltpu.with_memory_space_constraint(a, pltpu.HBM) if s is HBM else a for a, s in ins])


def weight_copies(hbm, buf, sems, row, rows):
    copies, at = [], 0
    for i, w in enumerate(hbm):
        cols = w.shape[1]
        copies.append(
            pltpu.make_async_copy(
                w.at[pl.ds(row, rows), :], buf.at[:, at : at + cols], sems.at[i]
            )
        )
        at += cols
    return copies


def tile_lanes(column, lanes):
    return jnp.concatenate([column] * (lanes // column.shape[1]), axis=1)


def block_mask(rows, row_step, lanes, lane_step):
    r = lax.broadcasted_iota(jnp.int32, (rows, lanes), 0) // row_step
    c = lax.broadcasted_iota(jnp.int32, (rows, lanes), 1) // lane_step
    return r == c


def own_half(tok_hbm, gain_hbm, extra_hbm, *refs):
    n = len(refs) - 11
    weights, (acc, xg, ssq, wide, ahead) = refs[:n], refs[n : n + 5]
    buf, sems, tok, gain, extra, small = refs[n + 5 :]
    tp = lax.axis_index("tp")
    half = tok.shape[1]
    here = pl.multiple_of(tp * half, half)
    away = pl.multiple_of((1 - tp) * half, half)
    loads = [
        pltpu.make_async_copy(src, dst, small.at[i])
        for i, (src, dst) in enumerate([(extra_hbm, extra), (gain_hbm, gain), (tok_hbm, tok)])
    ]
    copies = weight_copies(weights, buf, sems.at[0], here, half)
    more = weight_copies(weights, ahead, sems.at[1], away, half)
    for c in loads + copies:
        c.start()
    loads[0].wait()
    heads = extra.shape[0]
    lanes = wide.shape[1]
    r = lax.broadcasted_iota(jnp.int32, (heads, lanes), 0)
    c = lax.broadcasted_iota(jnp.int32, (heads, lanes), 1) // (lanes // heads)
    wide[...] = lax.dot_general(
        extra[...],
        (r == c).astype(F32),
        TN,
        precision=lax.Precision.HIGHEST,
        preferred_element_type=F32,
    )
    loads[1].wait()
    loads[2].wait()
    for c in more:
        c.start()
    x = tok[...].astype(F32)
    ssq[...] = jnp.broadcast_to(jnp.sum(x * x, axis=1, keepdims=True), ssq.shape)
    left = (x * gain[:, pl.ds(here, half)]).astype(BF16)
    xg[...] = left
    for c in copies:
        c.wait()
    acc[...] = dot(left, buf[...])
    for c in more:
        c.wait()


def other_half(
    tok, gain, bias, acc, xg, ssq, wide, wnext, full, scale, key, val, cum, base, send
):
    tp = lax.axis_index("tp")
    rows, half = tok.shape
    here = pl.multiple_of(tp * half, half)
    away = pl.multiple_of((1 - tp) * half, half)
    x = tok[...].astype(F32)
    power = (ssq[:, :1] + jnp.sum(x * x, axis=1, keepdims=True)) * (0.5 / half)
    r = jnp.broadcast_to(lax.rsqrt(power + NORM_EPS), scale.shape)
    scale[...] = r
    left = (x * gain[:, pl.ds(away, half)]).astype(BF16)
    full[:, pl.ds(away, half)] = left
    full[:, pl.ds(here, half)] = xg[...]

    def project(lo, hi):
        s = acc[:, lo:hi] + dot(left, wnext[:, lo:hi])
        return (s * tile_lanes(r, hi - lo)).astype(BF16)

    kw, vw = key.shape[1], val.shape[1]
    k = project(0, kw)
    key[...] = k
    f = project(kw, 2 * kw).astype(F32) + bias[...]
    log = (jnp.minimum(f, 0.0) - jnp.log1p(jnp.exp(-jnp.abs(f)))) * (1.0 / GATE_SOFTNESS)
    log = log + wide[...]
    hi = log.astype(BF16)
    rest = log - hi.astype(F32)
    mid = rest.astype(BF16)
    low = (rest - mid.astype(F32)).astype(BF16)
    tri = (
        lax.broadcasted_iota(jnp.int32, (BLOCK, 3 * BLOCK), 0)
        >= lax.broadcasted_iota(jnp.int32, (BLOCK, 3 * BLOCK), 1) % BLOCK
    ).astype(BF16)
    n = rows // BLOCK
    running = jnp.zeros((1, kw), F32)
    starts, parts = [], []
    for b in range(n):
        s = slice(b * BLOCK, (b + 1) * BLOCK)
        part = dot(tri, jnp.concatenate([hi[s], mid[s], low[s]], axis=0))
        cum[s, :] = part
        parts.append(part)
        starts.append(running)
        running = running + part[BLOCK - 1 :]
    base[...] = jnp.concatenate(starts + [running] * (base.shape[0] - n), axis=0)
    kf = k.astype(F32)
    decayed = []
    for b in range(n):
        s = slice(b * BLOCK, (b + 1) * BLOCK)
        decayed.append((kf[s] * jnp.exp((running - starts[b]) - parts[b])).astype(BF16))
    decayed = jnp.concatenate(decayed, axis=0)
    v = project(2 * kw, 2 * kw + vw)
    val[...] = v
    dv = send.shape[0] - EXTRA_ROWS
    states = []
    for g in range(vw // 256):
        m = lax.dot_general(
            v[:, g * 256 : (g + 1) * 256],
            decayed[:, g * 128 : (g + 1) * 128],
            TN,
            preferred_element_type=F32,
        )
        states.append(fold(m, dv))
    pack(send, jnp.concatenate(states, axis=1), jnp.exp(running))


def fold(m, dv):
    step = m.shape[1] // (m.shape[0] // dv)
    lane = lax.broadcasted_iota(jnp.int32, (dv, m.shape[1]), 1) // step
    out = m[:dv]
    for h in range(1, m.shape[0] // dv):
        out = jnp.where(lane == h, m[h * dv : (h + 1) * dv], out)
    return out


def pack(ref, state, decay, halo=None):
    dv = state.shape[0]
    ref[:dv, :] = state.astype(BF16)
    top = decay.astype(BF16).astype(F32)
    row = lax.broadcasted_iota(jnp.int32, (EXTRA_ROWS, state.shape[1]), 0)
    tail = jnp.where(row == 0, top, decay - top)
    if halo is not None:
        tail = jnp.where(row < 2, tail, halo)
    ref[dv:, :] = tail.astype(BF16)


def unpack(v, dv):
    tail = v[dv:].astype(F32)
    return v[:dv].astype(F32), tail[0:1] + tail[1:2], tail


def to_tail(last):
    width = last.shape[1] // 2
    row = lax.broadcasted_iota(jnp.int32, (EXTRA_ROWS, width), 0)
    tail = jnp.zeros((EXTRA_ROWS, width), F32)
    end = last.shape[0]
    for i in range(4):
        at = end - 2 + i // 2
        part = last[at : at + 1, (i % 2) * width : (i % 2 + 1) * width]
        tail = jnp.where(row == 2 + i, part, tail)
    return tail


def from_tail(tail):
    return jnp.concatenate(
        [
            jnp.concatenate([tail[2:3], tail[3:4]], axis=1),
            jnp.concatenate([tail[4:5], tail[5:6]], axis=1),
        ],
        axis=0,
    )


def fill(stack, items):
    for i, item in enumerate(items):
        stack[i] = item[...]


def halo_of_round(halo, stack, radix, stride, digit, dv):
    low_zero = lax.rem(lax.axis_index("sp"), stride) == 0
    for j in range(radix - 1):
        tail = stack[j ^ digit][dv:].astype(F32)
        halo = jnp.where((j + 1 == digit) & low_zero, tail, halo)
    return halo


def join_round(radix, stride, *refs):
    items, (sp, dp, cross, hp), (send, s_out, d_out, h_out), (stack,) = (
        refs[:radix],
        refs[radix : radix + 4],
        refs[radix + 4 : radix + 8],
        refs[radix + 8 :],
    )
    dv = sp.shape[0]
    fill(stack, items)
    digit = lax.rem(lax.axis_index("sp") // stride, radix)
    lanes = stack.shape[2]
    pre_s, pre_d = jnp.zeros((dv, lanes), F32), jnp.ones((1, lanes), F32)
    tot_s, tot_d = pre_s, pre_d
    for j in range(radix):
        s, d, tail = unpack(stack[j ^ digit], dv)
        before = j < digit
        pre_s = jnp.where(before, d * pre_s + s, pre_s)
        pre_d = jnp.where(before, d * pre_d, pre_d)
        tot_s, tot_d = d * tot_s + s, d * tot_d
    s_out[...] = dp[0:1] * pre_s + sp[...]
    d_out[...] = jnp.broadcast_to(dp[0:1] * pre_d, d_out.shape)
    if stride == 1:
        tail = to_tail(cross[...].astype(F32))
        h_out[...] = jnp.where(digit == 0, 0.0, tail)
    else:
        h_out[...] = halo_of_round(hp[...], stack, radix, stride, digit, dv)
    pack(send, tot_s, tot_d, tail)


def scaled(x, w, r):
    s = dot(x, w)
    return (s * tile_lanes(r, s.shape[1])).astype(BF16)


def conv_inputs(full, scale, wc, wh, prod, last):
    r = scale[...]
    x = full[...]
    p = scaled(x, wc[...], r).astype(F32) * scaled(x, wh[...], r).astype(F32)
    p = p.astype(BF16)
    prod[...] = p
    last[...] = p[p.shape[0] - last.shape[0] :]


def late_half(full, scale, taps, wb, wq, prod, query, outer, conv):
    r = scale[...]
    x = full[...]
    b = scaled(x, wb[...], r)
    outer[...] = b
    p = prod[...].astype(F32)
    row = lax.broadcasted_iota(jnp.int32, p.shape, 0)
    t = taps[...].astype(F32)
    total = jnp.zeros(p.shape, F32)
    for j in range(taps.shape[0] - 1):
        back = taps.shape[0] - 1 - j
        total = total + t[j : j + 1] * jnp.where(row >= back, pltpu.roll(p, back, 0), 0.0)
    total = total + t[taps.shape[0] - 1 :] * p
    conv[...] = (b.astype(F32) * total).astype(BF16)
    query[...] = scaled(x, wq[...], r)


def blockwise(
    key_dim, query, key, val, cum, base, start, full, scale, wg, gain, raw, through, first, gate
):
    rows = query.shape[0]
    n = rows // BLOCK
    shrink = key_dim**-0.5
    first[...] = start[...].T
    gated = scaled(full[...], wg[...], scale[...]).astype(F32)
    gate[...] = gated * jax.nn.sigmoid(gated) * tile_lanes(gain[...], gated.shape[1])
    k_mask = block_mask(256, 64, 128, 32)
    v_mask = block_mask(256, 64, 256, 64)
    causal = lax.broadcasted_iota(jnp.int32, (BLOCK, 256), 0) >= (
        lax.broadcasted_iota(jnp.int32, (BLOCK, 256), 1) % BLOCK
    )
    zero = jnp.zeros((), BF16)
    for g in range(val.shape[1] // 256):
        kl = slice(g * 128, (g + 1) * 128)
        vl = slice(g * 256, (g + 1) * 256)
        state = None
        for b in range(n):
            s = slice(b * BLOCK, (b + 1) * BLOCK)
            c = cum[s, kl]
            q = query[s, kl].astype(F32) * shrink
            k = key[s, kl].astype(F32)
            end = c[BLOCK - 1 :]
            q_in = (q * jnp.exp(c)).astype(BF16)
            k_in = (k * jnp.exp(-c)).astype(BF16)
            through[s, kl] = (q * jnp.exp(c + base[b : b + 1, kl])).astype(BF16)
            v = val[s, vl]
            k_wide = jnp.where(k_mask, jnp.concatenate([k_in] * 4, axis=0), zero)
            scores = lax.dot_general(q_in, k_wide, NT, preferred_element_type=F32)
            scores = jnp.where(causal, scores, 0.0).astype(BF16)
            v_wide = jnp.where(v_mask, jnp.concatenate([v] * 4, axis=0), zero)
            out = dot(scores, v_wide)
            if state is not None:
                out = out + lax.dot_general(
                    q_in, state.astype(BF16), NT, preferred_element_type=F32
                )
            raw[s, vl] = out
            if b < n - 1:
                k_out = (k * jnp.exp(end - c)).astype(BF16)
                new = lax.dot_general(v, k_out, TN, preferred_element_type=F32)
                new = jnp.where(k_mask, new, 0.0)
                state = new if state is None else state * jnp.exp(end) + new


def rows_out(half, incoming, halo, raw, through, gate, conv, outer, prod, taps):
    rows = raw.shape[0] // 2
    at = pl.multiple_of(half * rows, 64)
    here = pl.ds(at, rows)
    ones = block_mask(256, 64, 256, 64).astype(BF16) * (1.0 / 64)
    ones = ones.astype(BF16)
    parts = []
    for g in range(raw.shape[1] // 256):
        vl = slice(g * 256, (g + 1) * 256)
        x = raw[here, vl] + lax.dot_general(
            through[here, g * 128 : (g + 1) * 128],
            incoming[g],
            NT,
            preferred_element_type=F32,
        )
        mean = dot((x * x).astype(BF16), ones)
        parts.append((x * lax.rsqrt(mean + NORM_EPS) * gate[here, vl]).astype(BF16))
    attn = jnp.concatenate(parts, axis=1)
    p = prod[:16, :].astype(F32)
    row = lax.broadcasted_iota(jnp.int32, p.shape, 0)
    t = taps[...].astype(F32)
    back2 = jnp.where(row == 0, halo[0:1], jnp.where(row == 1, halo[1:2], pltpu.roll(p, 2, 0)))
    back1 = jnp.where(row == 0, halo[1:2], pltpu.roll(p, 1, 0))
    top = outer[:16, :].astype(F32) * (t[0:1] * back2 + t[1:2] * back1 + t[2:3] * p)
    mine = conv[here, :]
    head = jnp.where(half == 0, top, mine[:16].astype(F32)).astype(BF16)
    left = jnp.concatenate([head, mine[16:]], axis=0)
    return left, attn


def project_out(left, attn, wc, wa, out):
    step = 512
    for n in range(0, out.shape[1], step):
        s = dot(left, wc[:, n : n + step]) + dot(attn, wa[:, n : n + step])
        out[:, n : n + step] = s.astype(out.dtype)


def partner_rows(radix, stride, *refs):
    items = refs[:radix]
    sp, dp, hp, odd, first, raw, through, gate, conv, outer, prod, taps, wc, wa = refs[
        radix : radix + 14
    ]
    out, state, halo_out, stack = refs[radix + 14 :]
    dv = sp.shape[0]
    fill(stack, items)
    digit = lax.rem(lax.axis_index("sp") // stride, radix)
    lanes = stack.shape[2]
    pre_s = first[...]
    for j in range(radix - 1):
        s, d, _ = unpack(stack[j ^ digit], dv)
        pre_s = jnp.where(j < digit, d * pre_s + s, pre_s)
    pre_s = dp[0:1] * pre_s + sp[...]
    mask = block_mask(256, 64, 128, 32)
    incoming = []
    for g in range(lanes // 128):
        s = pre_s[:, g * 128 : (g + 1) * 128]
        wide = jnp.where(mask, jnp.concatenate([s] * 4, axis=0), 0.0).astype(BF16)
        incoming.append(wide)
        state[g] = wide
    halo = from_tail(halo_of_round(hp[...], stack, radix, stride, digit, dv))
    near = odd[...].astype(F32)[odd.shape[0] - 2 :]
    halo = jnp.where(lax.rem(lax.axis_index("sp"), 2) == 1, near, halo)
    halo_out[...] = jnp.concatenate([halo] * 4, axis=0)
    half = 1 - lax.axis_index("tp")
    left, attn = rows_out(half, incoming, halo, raw, through, gate, conv, outer, prod, taps)
    project_out(left, attn, wc, wa, out)


def own_rows(state, halo, raw, through, gate, conv, outer, prod, taps, wc, wa, out):
    incoming = [state[g] for g in range(state.shape[0])]
    half = lax.axis_index("tp")
    left, attn = rows_out(
        half, incoming, halo[0:2, :], raw, through, gate, conv, outer, prod, taps
    )
    project_out(left, attn, wc, wa, out)


def radices(n):
    found = []
    while n > 1:
        r = 4 if n % 4 == 0 else 2
        found.append(r)
        n //= r
    return found


def on_device(
    tokens,
    input_norm_gain,
    outer_gate_weight,
    inner_gate_weight,
    convolution_input_weight,
    convolution_kernel_taps,
    query_weight_matrix,
    key_weight_matrix,
    value_weight_matrix,
    forget_gate_weight,
    attention_gate_weight,
    forget_gate_bias,
    extra_logarithm_decay,
    initial_head_state,
    head_norm_gain,
    convolution_output_weight,
    attention_output_weight,
):
    rows, half = tokens.shape
    heads, dk, dv = initial_head_state.shape
    kw, vw, cw = heads * dk, heads * dv, outer_gate_weight.shape[1]
    model = convolution_output_weight.shape[1]
    n_sp = lax.axis_size("sp")
    swap = [(0, 1), (1, 0)]
    other = lax.ppermute(tokens, "tp", swap)
    gain = input_norm_gain.reshape(1, -1)
    early = (key_weight_matrix, forget_gate_weight, value_weight_matrix)
    width = sum(w.shape[1] for w in early)
    extra = extra_logarithm_decay.T
    flops = 2 * rows * half * width
    acc, xg, ssq, wide, ahead = call(
        own_half,
        [
            ((rows, width), F32),
            ((rows, half), BF16),
            ((rows, 128), F32),
            ((rows, kw), F32),
            ((half, width), BF16),
        ],
        [(tokens, HBM), (gain, HBM), (extra, HBM)] + [(w, HBM) for w in early],
        flops,
        [
            pltpu.VMEM((half, width), BF16),
            pltpu.SemaphoreType.DMA((2, len(early))),
            pltpu.VMEM(tokens.shape, BF16),
            pltpu.VMEM(gain.shape, F32),
            pltpu.VMEM(extra.shape, F32),
            pltpu.SemaphoreType.DMA((3,)),
        ],
    )
    full, scale, key, val, cum, base, send = call(
        other_half,
        [
            ((rows, 2 * half), BF16),
            ((rows, 128), F32),
            ((rows, kw), BF16),
            ((rows, vw), BF16),
            ((rows, kw), F32),
            ((8, kw), F32),
            ((dv + EXTRA_ROWS, kw), BF16),
        ],
        [(other, VMEM), (gain, VMEM), (forget_gate_bias.reshape(1, -1), VMEM)]
        + [(a, VMEM) for a in (acc, xg, ssq, wide, ahead)],
        flops,
    )
    prod, last = call(
        conv_inputs,
        [((rows, cw), BF16), ((16, cw), BF16)],
        [(a, VMEM) for a in (full, scale, inner_gate_weight, convolution_input_weight)],
        2 * rows * 2 * half * 2 * cw,
    )
    odd = lax.ppermute(last, "sp", [(i, i ^ 1) for i in range(n_sp)])
    cross = lax.ppermute(last, "sp", [(i, i ^ 3) for i in range(n_sp)])
    query, outer, conv = call(
        late_half,
        [((rows, kw), BF16), ((rows, cw), BF16), ((rows, cw), BF16)],
        [
            (a, VMEM)
            for a in (
                full,
                scale,
                convolution_kernel_taps,
                outer_gate_weight,
                query_weight_matrix,
                prod,
            )
        ],
        2 * rows * 2 * half * (kw + cw),
    )
    raw, through, first, gate = call(
        functools.partial(blockwise, dk),
        [((rows, vw), F32), ((rows, kw), BF16), ((dv, kw), F32), ((rows, vw), F32)],
        [
            (a, VMEM)
            for a in (
                query,
                key,
                val,
                cum,
                base,
                initial_head_state.reshape(heads * dk, dv),
                full,
                scale,
                attention_gate_weight,
                head_norm_gain.reshape(1, -1),
            )
        ],
        2 * rows * 2 * half * (kw + vw),
    )
    pre = (jnp.zeros((dv, kw), F32), jnp.ones((8, kw), F32))
    halo = jnp.zeros((EXTRA_ROWS, kw), F32)
    stride = 1
    plan = radices(n_sp)
    for turn, radix in enumerate(plan):
        items = [send]
        for j in range(1, radix):
            pairs = [(i, i ^ (j * stride)) for i in range(n_sp)]
            items.append(lax.ppermute(send, "sp", pairs))
        stack = [pltpu.VMEM((radix,) + send.shape, BF16)]
        if turn < len(plan) - 1:
            send, *pre, halo = call(
                functools.partial(join_round, radix, stride),
                [
                    (send.shape, BF16),
                    ((dv, kw), F32),
                    ((8, kw), F32),
                    ((EXTRA_ROWS, kw), F32),
                ],
                [(a, VMEM) for a in (*items, *pre, cross, halo)],
                1 << 20,
                stack,
            )
            stride *= radix
    tail = [
        (a, VMEM)
        for a in (
            raw,
            through,
            gate,
            conv,
            outer,
            prod,
            convolution_kernel_taps,
            convolution_output_weight,
            attention_output_weight,
        )
    ]
    flops = 2 * (rows // 2) * model * (vw + cw)
    theirs, state, halo = call(
        functools.partial(partner_rows, plan[-1], stride),
        [((rows // 2, model), BF16), ((kw // 128, 256, 128), BF16), ((8, cw), F32)],
        [(a, VMEM) for a in (*items, *pre, halo, odd, first)] + tail,
        flops,
        stack,
    )
    got = lax.ppermute(theirs, "tp", swap)
    (mine,) = call(
        own_rows,
        [((rows // 2, model), F32)],
        [(state, VMEM), (halo, VMEM)] + tail,
        flops,
    )
    return (mine + got.astype(F32)).astype(BF16)


def solution(mesh):
    placed = (
        P("sp", "tp"),
        P(),
        P(None, "tp"),
        P(None, "tp"),
        P(None, "tp"),
        P(None, "tp"),
        P(None, "tp"),
        P(None, "tp"),
        P(None, "tp"),
        P(None, "tp"),
        P(None, "tp"),
        P("tp"),
        P("sp", "tp"),
        P("tp", None, None),
        P(),
        P("tp", None),
        P("tp", None),
    )

    return jax.shard_map(
        on_device, mesh=mesh, in_specs=placed, out_specs=P(("sp", "tp"), None), check_vma=False
    )
```

time: 35.7 us -> 31.9 us (0.89)
  Pallas kernels: 18 us -> 13.4 us
  starting transfers between devices: 9.1 us -> 12.6 us
  waiting for transfers between devices: 7.03 us -> 4.36 us
    pallas_call x7 -> x8, Pallas kernels: 18 us -> 13.4 us  [call(): pl.pallas_call(body, out_shape=[jax.ShapeDtypeStruct(s, d) for s, d in ou...]
    ppermute x6 -> x8, starting transfers between devices: 8.54 us -> 12 us  [the longest x6 8.54 us: on_device(): items.append(lax.ppermute(send, 'sp', pairs))]
    ppermute x6 -> x8, waiting for transfers between devices: 6.55 us -> 3.33 us  [the longest x6 3.33 us: on_device(): items.append(lax.ppermute(send, 'sp', pairs))]
    ppermute x1, waiting for transfers between devices: 0.48 us -> 1.02 us  [on_device(): got = lax.ppermute(theirs, 'tp', swap)]
  transfers between devices with their start and end apart: 8 -> 10, of which waited for: 5 -> 3; matrix products, arithmetic and copies ran while one was open for 0% -> 0% of each run, Pallas kernels for 36% -> 32%
where the time goes in v3:
time: 31.9 us; the launch traced here: 31.8 us
  Pallas kernels  13.4 us (42%)
  starting transfers between devices  12.6 us (39%)
  waiting for transfers between devices  4.36 us (14%)
  other arithmetic  1.09 us (3%)
    pallas_call x8, Pallas kernels, call(): pl.pallas_call(body, out_shape=[jax.ShapeDtypeStruct(s, d) for s, d in ou...  13.4 us
    ppermute x6, starting transfers between devices, on_device(): items.append(lax.ppermute(send, 'sp', pairs))  8.54 us
    ppermute x6, waiting for transfers between devices, on_device(): items.append(lax.ppermute(send, 'sp', pairs))  3.33 us
    ppermute x1, starting transfers between devices, on_device(): cross = lax.ppermute(last, 'sp', [(i, i ^ 3) for i in range(n_sp)])  2.97 us
    convert_element_type x1, other arithmetic, on_device(): return (mine + got.astype(F32)).astype(BF16)  1.09 us
    ppermute x1, waiting for transfers between devices, on_device(): got = lax.ppermute(theirs, 'tp', swap)  1.02 us
  transfers between devices with their start and end apart: 10, of which 3 were waited for; matrix products, arithmetic and copies ran while one was open for 0% of the time, Pallas kernels for 32%

profile of v3, /device:TPU:0, one launch (start us, length us, event | category | flops | bytes accessed | tf_op | source)
XLA Modules:
  0.0 31.8 jit_solution(3841703574605694436)
XLA Ops:
  0.0 0.5 %collective-permute-start = (bf16[384,1024]{1,0:T(8,128)(2,1)}, bf16[384,1024]{1,0:T(8,128)(2,1)S(1)}, u32[]{:S(2)}, u32[]{:S(2)}) collective-permute-start(bf16[384,1024]{1,0:T(8,128)(2,1)} %tok_hbm.1), channel_id=1, source_target_pairs={{0,1},{1,0},{2,3},{3,2},{4,5},{5,4},{6,7},{7,6},{8,9},{9,8},{10,11... | collective-permute-start | bytes 2359304 | tf_op jit(solution)/shard_map/ppermute | solution.py:448
  0.5 0.0 copy-start.9
  0.5 3.2 %shard_map.163 = (f32[384,1024]{1,0:T(8,128)S(1)}, bf16[384,1024]{1,0:T(8,128)(2,1)S(1)}, f32[384,128]{1,0:T(8,128)S(1)}, f32[384,256]{1,0:T(8,128)S(1)}, bf16[1024,1024]{1,0:T(8,128)(2,1)S(1)}) custom-call(bf16[384,1024]{1,0:T(8,128)(2,1)} %tok_hbm.1, f32[1,2048]{1,0:T(1,128)} %bitcast.6, f32[8,384]{1,0:T(8,128)} %bitcast.10, bf16[2048,256]{1,0:T(8,128)(2,1)} %refs_0_.1, ...), custom_call_target="tpu_custom_call" | custom-call | flops 805306368 | bytes 1048576 | tf_op jit(solution)/shard_map/pallas_call | solution.py:29
  3.7 0.0 collective-permute-done.tok
  3.7 0.0 copy-done.9
  3.8 0.0 copy-done.10
  3.8 0.0 copy-start.2
  3.8 0.0 copy-start.3
  3.8 1.9 %shard_map.164 = (bf16[384,2048]{1,0:T(8,128)(2,1)S(1)}, f32[384,128]{1,0:T(8,128)S(1)}, bf16[384,256]{1,0:T(8,128)(2,1)S(1)}, bf16[384,512]{1,0:T(8,128)(2,1)S(...) custom-call(bf16[384,1024]{1,0:T(8,128)(2,1)S(1)} %collective-permute-done.tok, ...), custom_call_target="tpu_custom_call" | custom-call | flops 805306368 | bytes 1048576 | tf_op jit(solution)/shard_map/pallas_call | solution.py:29
  5.7 2.5 %collective-permute-start.1 = (bf16[80,256]{1,0:T(8,128)(2,1)S(1)}, bf16[80,256]{1,0:T(8,128)(2,1)S(1)}, u32[]{:S(2)}, u32[]{:S(2)}) collective-permute-start(bf16[80,256]{1,0:T(8,128)(2,1)S(1)} %get-tuple-element.38.refs_0_), channel_id=1, source_target_pairs={{0,2},{2,0},{4,6},{6,4},{8,10},{10,8},{12,14},{14,12},{16,18},{18,... | collective-permute-start | bytes 122888 | tf_op jit(solution)/shard_map/ppermute | solution.py:541
  8.2 1.5 %collective-permute-start.2 = (bf16[80,256]{1,0:T(8,128)(2,1)S(1)}, bf16[80,256]{1,0:T(8,128)(2,1)S(1)}, u32[]{:S(2)}, u32[]{:S(2)}) collective-permute-start(bf16[80,256]{1,0:T(8,128)(2,1)S(1)} %get-tuple-element.38.refs_0_), channel_id=1, source_target_pairs={{0,4},{2,6},{4,0},{6,2},{8,12},{10,14},{12,8},{14,10},{16,20},{18,... | collective-permute-start | bytes 122888 | tf_op jit(solution)/shard_map/ppermute | solution.py:541
  9.7 0.0 collective-permute-start.3
  9.8 0.0 copy-done.2
  9.8 0.0 copy-done.3
  9.8 0.0 copy-start.8
  9.8 1.8 %shard_map.165 = (bf16[384,512]{1,0:T(8,128)(2,1)S(1)}, bf16[16,512]{1,0:T(8,128)(2,1)S(1)}) custom-call(bf16[384,2048]{1,0:T(8,128)(2,1)S(1)} %get-tuple-element.39.full, f32[384,128]{1,0:T(8,128)S(1)} %get-tuple-element.40.scale, bf16[2048,512]{1,0:T(8,128)(2,1)S(1)} %copy-done.2, bf16[2048,512]{1,0:T(8,128)(2,1)S(1)} %copy-done.3), custom_call_target="tpu_custom_call" | custom-call | flops 1610612736 | bytes 1048576 | tf_op jit(solution)/shard_map/pallas_call | solution.py:29
  11.6 3.0 %collective-permute-start.4 = (bf16[16,512]{1,0:T(8,128)(2,1)S(1)}, bf16[16,512]{1,0:T(8,128)(2,1)S(1)}, u32[]{:S(2)}, u32[]{:S(2)}) collective-permute-start(bf16[16,512]{1,0:T(8,128)(2,1)S(1)} %get-tuple-element.41), channel_id=1, source_target_pairs={{0,6},{2,4},{4,2},{6,0},{8,14},{10,12},{12,10},{14,8},{16,22},{18,... | collective-permute-start | bytes 49160 | tf_op jit(solution)/shard_map/ppermute | solution.py:496
  14.6 0.5 %collective-permute-start.8 = (bf16[16,512]{1,0:T(8,128)(2,1)S(1)}, bf16[16,512]{1,0:T(8,128)(2,1)S(1)}, u32[]{:S(2)}, u32[]{:S(2)}) collective-permute-start(bf16[16,512]{1,0:T(8,128)(2,1)S(1)} %get-tuple-element.41), channel_id=1, source_target_pairs={{0,2},{2,0},{4,6},{6,4},{8,10},{10,8},{12,14},{14,12},{16,18},{18,... | collective-permute-start | bytes 49160 | tf_op jit(solution)/shard_map/ppermute | solution.py:495
  15.1 0.0 copy-done.4
  15.1 0.0 copy-done.6
  15.1 0.0 copy-done.8
  15.1 0.0 copy-start.7
  15.2 0.0 copy-start.11
  15.2 1.5 %shard_map.167 = (bf16[384,256]{1,0:T(8,128)(2,1)S(1)}, bf16[384,512]{1,0:T(8,128)(2,1)S(1)}, bf16[384,512]{1,0:T(8,128)(2,1)S(1)}) custom-call(bf16[384,2048]{1,0:T(8,128)(2,1)S(1)} %get-tuple-element.39.full, f32[384,128]{1,0:T(8,128)S(1)} %get-tuple-element.40.scale, bf16[3,512]{1,0:T(4,128)(2,1)S(1)} %copy-done.8, bf16[2048,512]{1,0:T(8,128)(2,1)S(1)} %copy-done.4, ...), custom_call_target="tpu_custom_call" | custom-call | flops 1207959552 | bytes 1048576 | tf_op jit(solution)/shard_map/pallas_call | solution.py:29
  16.6 0.0 collective-permute-done.4.refs_6_
  16.7 0.0 collective-permute-done.1.refs_1_
  16.7 0.0 collective-permute-done.2.refs_2_
  16.7 0.0 collective-permute-done.3.refs_3_
  16.7 0.1 shard_map.166
  16.8 1.8 %collective-permute-start.5 = (bf16[80,256]{1,0:T(8,128)(2,1)S(1)}, bf16[80,256]{1,0:T(8,128)(2,1)S(1)}, u32[]{:S(2)}, u32[]{:S(2)}) collective-permute-start(bf16[80,256]{1,0:T(8,128)(2,1)S(1)} %get-tuple-element.42.refs_0_), channel_id=1, source_target_pairs={{0,8},{2,10},{4,12},{6,14},{8,0},{10,2},{12,4},{14,6},{16,24},{18,... | collective-permute-start | bytes 122888 | tf_op jit(solution)/shard_map/ppermute | solution.py:541
  18.6 2.6 %collective-permute-start.6 = (bf16[80,256]{1,0:T(8,128)(2,1)S(1)}, bf16[80,256]{1,0:T(8,128)(2,1)S(1)}, u32[]{:S(2)}, u32[]{:S(2)}) collective-permute-start(bf16[80,256]{1,0:T(8,128)(2,1)S(1)} %get-tuple-element.42.refs_0_), channel_id=1, source_target_pairs={{0,16},{2,18},{4,20},{6,22},{8,24},{10,26},{12,28},{14,30},{16,0},... | collective-permute-start | bytes 122888 | tf_op jit(solution)/shard_map/ppermute | solution.py:541
  21.2 0.0 collective-permute-start.7
  21.3 0.0 copy-done.5
  21.3 0.0 copy-done.7
  21.3 0.0 copy-done.11
  21.3 0.0 copy-start.1
  21.3 2.4 %shard_map.168 = (f32[384,512]{1,0:T(8,128)S(1)}, bf16[384,256]{1,0:T(8,128)(2,1)S(1)}, f32[64,256]{1,0:T(8,128)S(1)}, f32[384,512]{1,0:T(8,128)S(1)}) custom-call(bf16[384,256]{1,0:T(8,128)(2,1)S(1)} %get-tuple-element.47.query, bf16[384,256]{1,0:T(8,128)(2,1)S(1)} %get-tuple-element.48.key, bf16[384,512]{1,0:T(8,128)(2,1)S(1)} %get-tuple-element.49.val, ...), custom_call_target="tpu_custom_call" | custom-call | flops 1207959552 | bytes 1048576 | tf_op jit(solution)/shard_map/pallas_call | solution.py:29
  23.7 0.0 collective-permute-done.8.refs_7_
  23.7 0.0 collective-permute-done.5.refs_1_
  23.7 0.3 collective-permute-done.6.refs_2_
  24.0 3.1 %collective-permute-done.7.refs_3_ = bf16[80,256]{1,0:T(8,128)(2,1)S(1)} collective-permute-done((bf16[80,256]{1,0:T(8,128)(2,1)S(1)}, bf16[80,256]{1,0:T(8,128)(2,1)S(1)}, u32[]{:S(2)}, u32[]{:S(2)}) %collective-permute-start.7) | collective-permute-done | bytes 40992 | tf_op jit(solution)/shard_map/ppermute | solution.py:541
  27.0 0.0 copy-done
  27.0 0.0 copy-done.1
  27.0 1.3 %shard_map.169 = (bf16[192,2048]{1,0:T(8,128)(2,1)S(1)}, bf16[2,256,128]{2,1,0:T(8,128)(2,1)S(1)}, f32[8,512]{1,0:T(8,128)S(1)}) custom-call(bf16[80,256]{1,0:T(8,128)(2,1)S(1)} %get-tuple-element.42.refs_0_, bf16[80,256]{1,0:T(8,128)(2,1)S(1)} %collective-permute-done.5.refs_1_, bf16[80,256]{1,0:T(8,128)(2,1)S(1)} %collective-permute-done.6.refs_2_, ...), custom_call_target="tpu_custom_call" | custom-call | flops 805306368 | bytes 1048576 | tf_op jit(solution)/shard_map/pallas_call | solution.py:29
  28.3 0.1 collective-permute-start.9
  28.4 1.2 %shard_map.170 = f32[192,2048]{1,0:T(8,128)S(1)} custom-call(bf16[2,256,128]{2,1,0:T(8,128)(2,1)S(1)} %get-tuple-element.58.state, f32[8,512]{1,0:T(8,128)S(1)} %get-tuple-element.59.halo, f32[384,512]{1,0:T(8,128)S(1)} %get-tuple-element.53.refs_9_.raw, bf16[384,256]{1,0:T(8,128)(2,1)S(1)} %get-tuple-element.54.refs_10_.through, ...), custom_call_target="tpu_custom_call" | custom-call | flops 805306368 | bytes 1048576 | tf_op jit(solution)/shard_map/pallas_call | solution.py:29
  29.7 1.0 %collective-permute-done.9 = bf16[192,2048]{1,0:T(8,128)(2,1)S(1)} collective-permute-done((bf16[192,2048]{1,0:T(8,128)(2,1)S(1)}, bf16[192,2048]{1,0:T(8,128)(2,1)S(1)}, u32[]{:S(2)}, u32[]{:S(2)}) %collective-permute-start.9) | collective-permute-done | bytes 786464 | tf_op jit(solution)/shard_map/ppermute | solution.py:579
  30.7 1.1 %add_convert_fusion = bf16[192,2048]{1,0:T(8,128)(2,1)} fusion(f32[192,2048]{1,0:T(8,128)S(1)} %shard_map.170, bf16[192,2048]{1,0:T(8,128)(2,1)S(1)} %collective-permute-done.9), kind=kLoop, calls=%fused_computation | loop fusion | flops 1179648 | bytes 3145728 | tf_op jit(solution)/shard_map/convert_element_type | solution.py:586
  (8 shorter events, 0.0 us)
Async XLA Ops:
  0.0 3.7 %collective-permute-start = (bf16[384,1024]{1,0:T(8,128)(2,1)}, bf16[384,1024]{1,0:T(8,128)(2,1)S(1)}, u32[]{:S(2)}, u32[]{:S(2)}) collective-permute-start(bf16[384,1024]{1,0:T(8,128)(2,1)} %tok_hbm.1), channel_id=1, source_target_pairs={{0,1},{1,0},{2,3},{3,2},{4,5},{5,4},{6,7},{7,6},{8,9},{9,8},{10,11... | collective-permute-start | bytes 2359304 | tf_op jit(solution)/shard_map/ppermute | solution.py:448
  0.5 3.2 %copy-start.9 = (f32[2048]{0:T(1024)S(1)}, f32[2048]{0:T(1024)}, u32[]{:S(2)}) copy-start(f32[2048]{0:T(1024)} %param.18) | copy-start | bytes 24580
  0.5 3.3 %copy-start.10 = (f32[256]{0:T(256)S(1)}, f32[256]{0:T(256)}, u32[]{:S(2)}) copy-start(f32[256]{0:T(256)} %param.28) | copy-start | bytes 3076
  3.8 6.0 %copy-start.2 = (bf16[2048,512]{1,0:T(8,128)(2,1)S(1)}, bf16[2048,512]{1,0:T(8,128)(2,1)}, u32[]{:S(2)}) copy-start(bf16[2048,512]{1,0:T(8,128)(2,1)} %wc.2) | copy-start | bytes 6291460
  3.8 6.0 %copy-start.3 = (bf16[2048,512]{1,0:T(8,128)(2,1)S(1)}, bf16[2048,512]{1,0:T(8,128)(2,1)}, u32[]{:S(2)}) copy-start(bf16[2048,512]{1,0:T(8,128)(2,1)} %wh.1) | copy-start | bytes 6291460
  5.7 11.0 %collective-permute-start.1 = (bf16[80,256]{1,0:T(8,128)(2,1)S(1)}, bf16[80,256]{1,0:T(8,128)(2,1)S(1)}, u32[]{:S(2)}, u32[]{:S(2)}) collective-permute-start(bf16[80,256]{1,0:T(8,128)(2,1)S(1)} %get-tuple-element.38.refs_0_), channel_id=1, source_target_pairs={{0,2},{2,0},{4,6},{6,4},{8,10},{10,8},{12,14},{14,12},{16,18},{18,... | collective-permute-start | bytes 122888 | tf_op jit(solution)/shard_map/ppermute | solution.py:541
  8.2 8.5 %collective-permute-start.2 = (bf16[80,256]{1,0:T(8,128)(2,1)S(1)}, bf16[80,256]{1,0:T(8,128)(2,1)S(1)}, u32[]{:S(2)}, u32[]{:S(2)}) collective-permute-start(bf16[80,256]{1,0:T(8,128)(2,1)S(1)} %get-tuple-element.38.refs_0_), channel_id=1, source_target_pairs={{0,4},{2,6},{4,0},{6,2},{8,12},{10,14},{12,8},{14,10},{16,20},{18,... | collective-permute-start | bytes 122888 | tf_op jit(solution)/shard_map/ppermute | solution.py:541
  9.7 6.9 %collective-permute-start.3 = (bf16[80,256]{1,0:T(8,128)(2,1)S(1)}, bf16[80,256]{1,0:T(8,128)(2,1)S(1)}, u32[]{:S(2)}, u32[]{:S(2)}) collective-permute-start(bf16[80,256]{1,0:T(8,128)(2,1)S(1)} %get-tuple-element.38.refs_0_), channel_id=1, source_target_pairs={{0,6},{2,4},{4,2},{6,0},{8,14},{10,12},{12,10},{14,8},{16,22},{18,... | collective-permute-start | bytes 122888 | tf_op jit(solution)/shard_map/ppermute | solution.py:541
  9.8 5.4 %copy-start.4 = (bf16[2048,512]{1,0:T(8,128)(2,1)S(1)}, bf16[2048,512]{1,0:T(8,128)(2,1)}, u32[]{:S(2)}) copy-start(bf16[2048,512]{1,0:T(8,128)(2,1)} %wb.1) | copy-start | bytes 6291460
  9.8 5.4 %copy-start.6 = (bf16[2048,256]{1,0:T(8,128)(2,1)S(1)}, bf16[2048,256]{1,0:T(8,128)(2,1)}, u32[]{:S(2)}) copy-start(bf16[2048,256]{1,0:T(8,128)(2,1)} %wq.1) | copy-start | bytes 3145732
  9.8 5.4 %copy-start.8 = (bf16[3,512]{1,0:T(4,128)(2,1)S(1)}, bf16[3,512]{1,0:T(4,128)(2,1)}, u32[]{:S(2)}) copy-start(bf16[3,512]{1,0:T(4,128)(2,1)} %taps.3) | copy-start | bytes 9220
  11.6 5.0 %collective-permute-start.4 = (bf16[16,512]{1,0:T(8,128)(2,1)S(1)}, bf16[16,512]{1,0:T(8,128)(2,1)S(1)}, u32[]{:S(2)}, u32[]{:S(2)}) collective-permute-start(bf16[16,512]{1,0:T(8,128)(2,1)S(1)} %get-tuple-element.41), channel_id=1, source_target_pairs={{0,6},{2,4},{4,2},{6,0},{8,14},{10,12},{12,10},{14,8},{16,22},{18,... | collective-permute-start | bytes 49160 | tf_op jit(solution)/shard_map/ppermute | solution.py:496
  14.6 9.1 %collective-permute-start.8 = (bf16[16,512]{1,0:T(8,128)(2,1)S(1)}, bf16[16,512]{1,0:T(8,128)(2,1)S(1)}, u32[]{:S(2)}, u32[]{:S(2)}) collective-permute-start(bf16[16,512]{1,0:T(8,128)(2,1)S(1)} %get-tuple-element.41), channel_id=1, source_target_pairs={{0,2},{2,0},{4,6},{6,4},{8,10},{10,8},{12,14},{14,12},{16,18},{18,... | collective-permute-start | bytes 49160 | tf_op jit(solution)/shard_map/ppermute | solution.py:495
  15.1 6.1 %copy-start.5 = (bf16[2048,512]{1,0:T(8,128)(2,1)S(1)}, bf16[2048,512]{1,0:T(8,128)(2,1)}, u32[]{:S(2)}) copy-start(bf16[2048,512]{1,0:T(8,128)(2,1)} %wg.1) | copy-start | bytes 6291460
  15.1 6.1 %copy-start.7 = (f32[8,32,64]{2,1,0:T(8,128)S(1)}, f32[8,32,64]{2,1,0:T(8,128)}, u32[]{:S(2)}) copy-start(f32[8,32,64]{2,1,0:T(8,128)} %param.30) | copy-start | bytes 196612
  15.2 6.1 %copy-start.11 = (f32[64]{0:T(128)S(1)}, f32[64]{0:T(128)}, u32[]{:S(2)}) copy-start(f32[64]{0:T(128)} %param.31) | copy-start | bytes 772
  16.8 6.9 %collective-permute-start.5 = (bf16[80,256]{1,0:T(8,128)(2,1)S(1)}, bf16[80,256]{1,0:T(8,128)(2,1)S(1)}, u32[]{:S(2)}, u32[]{:S(2)}) collective-permute-start(bf16[80,256]{1,0:T(8,128)(2,1)S(1)} %get-tuple-element.42.refs_0_), channel_id=1, source_target_pairs={{0,8},{2,10},{4,12},{6,14},{8,0},{10,2},{12,4},{14,6},{16,24},{18,... | collective-permute-start | bytes 122888 | tf_op jit(solution)/shard_map/ppermute | solution.py:541
  18.6 5.3 %collective-permute-start.6 = (bf16[80,256]{1,0:T(8,128)(2,1)S(1)}, bf16[80,256]{1,0:T(8,128)(2,1)S(1)}, u32[]{:S(2)}, u32[]{:S(2)}) collective-permute-start(bf16[80,256]{1,0:T(8,128)(2,1)S(1)} %get-tuple-element.42.refs_0_), channel_id=1, source_target_pairs={{0,16},{2,18},{4,20},{6,22},{8,24},{10,26},{12,28},{14,30},{16,0},... | collective-permute-start | bytes 122888 | tf_op jit(solution)/shard_map/ppermute | solution.py:541
  21.2 5.8 %collective-permute-start.7 = (bf16[80,256]{1,0:T(8,128)(2,1)S(1)}, bf16[80,256]{1,0:T(8,128)(2,1)S(1)}, u32[]{:S(2)}, u32[]{:S(2)}) collective-permute-start(bf16[80,256]{1,0:T(8,128)(2,1)S(1)} %get-tuple-element.42.refs_0_), channel_id=1, source_target_pairs={{0,24},{2,26},{4,28},{6,30},{8,16},{10,18},{12,20},{14,22},{16,8},... | collective-permute-start | bytes 122888 | tf_op jit(solution)/shard_map/ppermute | solution.py:541
  21.3 5.8 %copy-start = (bf16[512,2048]{1,0:T(8,128)(2,1)S(1)}, bf16[512,2048]{1,0:T(8,128)(2,1)}, u32[]{:S(2)}) copy-start(bf16[512,2048]{1,0:T(8,128)(2,1)} %wc.3) | copy-start | bytes 6291460
  21.3 5.8 %copy-start.1 = (bf16[512,2048]{1,0:T(8,128)(2,1)S(1)}, bf16[512,2048]{1,0:T(8,128)(2,1)}, u32[]{:S(2)}) copy-start(bf16[512,2048]{1,0:T(8,128)(2,1)} %wa.1) | copy-start | bytes 6291460
  28.3 2.4 %collective-permute-start.9 = (bf16[192,2048]{1,0:T(8,128)(2,1)S(1)}, bf16[192,2048]{1,0:T(8,128)(2,1)S(1)}, u32[]{:S(2)}, u32[]{:S(2)}) collective-permute-start(bf16[192,2048]{1,0:T(8,128)(2,1)S(1)} %get-tuple-element.60), channel_id=1, source_target_pairs={{0,1},{1,0},{2,3},{3,2},{4,5},{5,4},{6,7},{7,6},{8,9},{9,8},{10,11... | collective-permute-start | bytes 2359304 | tf_op jit(solution)/shard_map/ppermute | solution.py:579
